TPU v7x, 256 devices: a whole 4x4x8 slice. The times are simulated.
256 devices in a mesh: sp: 16 (over y, x), tp: 16 (over z, core).
Axes of the slice: x: 4, y: 4, z: 8, core: 2. Of those that a mesh axis runs over, the one named last changes fastest.
Arguments:
- ask_preactivation_left: bfloat16 [8192, 2048], P('sp', 'tp'), may hold values from -6 to 6
- keep_preactivation_left: bfloat16 [8192, 2048], P('sp', 'tp'), may hold values from -6 to 6
- keep_bound_complement_left: float32 [2048], P('tp'), may hold values from 0 to 0.1
- ask_preactivation_right: bfloat16 [8192, 4096], P('sp', 'tp'), may hold values from -6 to 6
- keep_preactivation_right: bfloat16 [8192, 4096], P('sp', 'tp'), may hold values from -6 to 6
- keep_bound_complement_right: float32 [4096], P('tp'), may hold values from 0 to 0.1
- payload_entries: bfloat16 [8192, 2048], P('sp', 'tp'), may hold values from -6 to 6
- emission_switch_logits: bfloat16 [8192, 2048], P('sp', 'tp'), may hold values from -6 to 6
- added_log_keep_bias: float32 [8192, 32], P('sp', 'tp'), may hold values from -2.1 to 0
- lanewise_rescale: float32 [64], replicated, may hold values from 0.1 to 1.9
- emission_matrix_alpha: bfloat16 [1024, 2048], P('tp'), may hold values from -0.125 to 0.125
- emission_matrix_beta: bfloat16 [1024, 2048], P('tp'), may hold values from -0.125 to 0.125
- skip_stream: bfloat16 [8192, 2048], P(('sp', 'tp')), may hold values from -6 to 6
- postrecurrence_rescale: float32 [2048], replicated, may hold values from 0.1 to 1.9
- premixture_rescale: float32 [2048], replicated, may hold values from 0.1 to 1.9
- postmixture_rescale: float32 [2048], replicated, may hold values from 0.1 to 1.9
- dispatcher_columns: bfloat16 [2048, 32], P(None, 'sp'), may hold values from -0.125 to 0.125
- switch_matrix: bfloat16 [16, 2048, 4096], P('sp', None, 'tp'), may hold values from -0.125 to 0.125
- expansion_matrix: bfloat16 [16, 2048, 4096], P('sp', None, 'tp'), may hold values from -0.125 to 0.125
- contraction_matrix: bfloat16 [16, 4096, 2048], P('sp', 'tp'), may hold values from -0.125 to 0.125
- item_specialist_cluster: int32 [8192], P(('sp', 'tp')), may hold values from 0 to 15, as said below
Outputs:
- result: bfloat16 [8192, 2048], P(('sp', 'tp'))
Inputs may be any that keep to these rules, and one draw needn't show every extreme that they name: `item_specialist_cluster`: in every aligned block of 32 tokens (the rows of one device) no group is named more than 3 times, and some group exactly 3 times.
All inputs are finite; a program needn't handle non-finite values.
Results may differ from a plain program's by a relative error of at most 0.023.
Values may be sent and summed in bfloat16 or wider, within the bound.
No kernel may reach another device: no remote copies, remote signals or barrier semaphores. Data moves between devices by JAX's collectives and lax.ppermute only.
A program may use at most 64 MiB of HBM per device.

v0:
```python
import jax
import jax.numpy as jnp
from jax import lax
from jax.experimental import pallas as pl
from jax.experimental.pallas import tpu as pltpu
from jax.sharding import Mesh, PartitionSpec as P


EPSILON = 1e-06
F32 = jnp.float32
BF16 = jnp.bfloat16
VMEM = pl.BlockSpec(memory_space=pltpu.VMEM)
SMEM = pl.BlockSpec(memory_space=pltpu.SMEM)
HBM = pl.BlockSpec(memory_space=pltpu.HBM)


def shifted(v, axis, by):
    n = lax.axis_size(axis)
    return lax.ppermute(v, axis, [(i, (i + by) % n) for i in range(n)])


def partner(v):
    return lax.ppermute(v, "core", [(0, 1), (1, 0)])


def dot(a, b):
    return jnp.dot(a, b, preferred_element_type=F32)


def dot_t(a, b):
    return lax.dot_general(a, b, (((1,), (1,)), ((), ())), preferred_element_type=F32)


def dot_0(a, b):
    return lax.dot_general(a, b, (((0,), (0,)), ((), ())), preferred_element_type=F32)


def rms_scale(features, gain):
    return (
        features * lax.rsqrt(jnp.mean(features * features, axis=-1, keepdims=True) + EPSILON) * gain
    )


def call(body, outs, args, scratch=(), specs=None, flops=0, moved=0, limit=4):
    return pl.pallas_call(
        body,
        out_shape=outs,
        in_specs=specs or [VMEM] * len(args),
        out_specs=jax.tree.map(lambda _: VMEM, outs),
        scratch_shapes=list(scratch),
        cost_estimate=pl.CostEstimate(flops=flops, bytes_accessed=moved, transcendentals=0),
        compiler_params=pltpu.CompilerParams(vmem_limit_bytes=limit << 20),
    )(*args)


def neighbour(v):
    return lax.ppermute(v, "z", [(i, i ^ 1) for i in range(8)])


def from_stride(outs):
    return (outs[0], shifted(outs[1], "z", 2), shifted(outs[3], "z", -2), shifted(outs[2], "z", 4))


def ring_gather(chunk):
    below, above = [chunk], [chunk]
    for _ in range(3):
        below.append(shifted(below[-1], "z", 1))
        above.append(shifted(above[-1], "z", -1))
    far = shifted(below[3], "z", 1)
    return [*above, far, *below[:0:-1]]


def unpack(ref):
    wide = ref[...].astype(F32)
    return wide[:64], wide[64:65] + wide[65:66]


def pack(ref, lanes, state, total):
    hi = total.astype(BF16).astype(F32)
    row = lax.broadcasted_iota(jnp.int32, (16, total.shape[1]), 0)
    tail = jnp.where(row == 0, hi, jnp.where(row == 1, total - hi, 0.0))
    ref[:64, lanes] = state.astype(BF16)
    ref[64:, lanes] = tail.astype(BF16)


def prefix_of(pieces, places, limit):
    state, total = 0.0, 0.0
    for (s_k, l_k), p_k in zip(pieces, places):
        later = jnp.zeros_like(l_k)
        for (_, l_m), p_m in zip(pieces, places):
            later = later + jnp.where((p_m > p_k) & (p_m < limit), l_m, 0.0)
        use = p_k < limit
        state = state + jnp.where(use, jnp.exp(later) * s_k, 0.0)
        total = total + jnp.where(use, l_k, 0.0)
    return state, total


SIDES = (slice(0, 128), slice(128, 384))


def prepare_body(*refs):
    far, (ga, gb, bias), refs = refs[:7], refs[7:10], refs[10:]
    packed, q_dec, k_grown, weights, qa, fa, qb, fb, values, sems = refs
    near = (qa, fa, qb, fb, values, weights.at[:64], weights.at[64:])
    copies = [
        pltpu.make_async_copy(src, dst, sems.at[i]) for i, (src, dst) in enumerate(zip(far, near))
    ]
    for i in (1, 3, 4, 0, 2, 5, 6):
        copies[i].start()
    rows = qa.shape[0]
    at = lax.broadcasted_iota(jnp.int32, (rows, rows), 0)
    of = lax.broadcasted_iota(jnp.int32, (rows, rows), 1)
    ones = jnp.where(at >= of, 1.0, 0.0)
    biases = [
        jnp.sum(ones * bias[side : side + 1, :], axis=1, keepdims=True) for side in (0, 1)
    ]
    ones = ones.astype(BF16)
    copies[4].wait()
    flipped = values[...].astype(F32).T.astype(BF16)
    for side, (q, f, g, lanes) in enumerate(((qa, fa, ga, SIDES[0]), (qb, fb, gb, SIDES[1]))):
        copies[2 * side + 1].wait()
        key = g[...] * jax.nn.sigmoid(-f[...].astype(F32))
        logf = jnp.log1p(-key)
        hi = logf.astype(BF16)
        lo = (logf - hi.astype(F32)).astype(BF16)
        inside = dot(ones, hi) + dot(ones, lo) + biases[side]
        total = inside[rows - 1 : rows]
        k_last = (key * jnp.exp(total - inside)).astype(BF16)
        pack(packed, lanes, dot(flipped[64 * side : 64 * side + 64], k_last), total)
        copies[2 * side].wait()
        q_dec[:, lanes] = (jax.nn.silu(q[...].astype(F32)) * jnp.exp(inside)).astype(BF16)
        k_grown[:, lanes] = (key * jnp.exp(-inside)).astype(BF16)
    copies[5].wait()
    copies[6].wait()


def inner_body(q_dec, k_grown, values, intra):
    rows = q_dec.shape[0]
    at = lax.broadcasted_iota(jnp.int32, (rows, rows), 0)
    of = lax.broadcasted_iota(jnp.int32, (rows, rows), 1)
    for side, lanes in enumerate(SIDES):
        cols = slice(64 * side, 64 * side + 64)
        scores = jnp.where(at >= of, dot_t(q_dec[:, lanes], k_grown[:, lanes]), 0.0).astype(BF16)
        intra[:, cols] = dot(scores, values[:, cols])


def spread_body(at, own, got1, got2, got3, sent, before):
    x = at[0]
    row = [unpack(ref) for ref in (own, got1, got2, got3)]
    places = [(x + 4 - k) % 4 for k in range(4)]
    pack(sent, slice(None), *prefix_of(row, places, 4))
    state, total = prefix_of(row, places, x)
    before[:64, :] = state
    before[64:, :] = jnp.broadcast_to(total, (8, total.shape[1]))


def head_body(at, q_dec, before, got1, got2, got3, intra, gates, gain, keep, give, heads):
    y = at[3]
    rows_above = [unpack(ref) for ref in (got1, got2, got3)]
    above, _ = prefix_of(rows_above, [(y + 4 - k) % 4 for k in (1, 2, 3)], y)
    carried = (jnp.exp(before[64:65, :]) * above + before[:64, :]).astype(BF16)
    for side, lanes in enumerate(SIDES):
        cols = slice(64 * side, 64 * side + 64)
        raw = intra[:, cols] + dot_t(q_dec[:, lanes], carried[:, lanes])
        gate = jax.nn.sigmoid(gates[:, cols].astype(F32))
        heads[:, cols] = rms_scale(raw, gain[...]) * gate
    z, core = at[1], at[2]
    for out, whose in ((keep, core), (give, 1 - core)):
        for r in range(8):
            block = 2 * ((z + r) % 8) + whose
            rows = heads[pl.ds(pl.multiple_of(block * 32, 32), 32), :]
            out[32 * r : 32 * r + 32, :] = rows.astype(BF16)


def heads_of(qa, fa, gap_a, qb, fb, gap_b, values, gates, bias, gain, w_a, w_b):
    rows = qa.shape[0]
    packed_shape = jax.ShapeDtypeStruct((80, 384), BF16)
    wide = jax.ShapeDtypeStruct((rows, 384), BF16)
    far = (qa, fa, qb, fb, values, w_a, w_b)
    packed, q_dec, k_grown, w_own = call(
        prepare_body,
        (packed_shape, wide, wide, jax.ShapeDtypeStruct((128, 2048), BF16)),
        (*far, gap_a[None], gap_b[None], bias.T),
        scratch=[*(pltpu.VMEM(v.shape, BF16) for v in far[:5]), pltpu.SemaphoreType.DMA((7,))],
        specs=[HBM] * 7 + [VMEM] * 3,
        flops=6 * rows * rows * 384,
        moved=3 << 20,
        limit=60,
    )
    at = jnp.stack([lax.axis_index(name) for name in ("x", "z", "core", "y")])
    row = [shifted(packed, "x", k) for k in (1, 2, 3)]
    intra = call(
        inner_body,
        jax.ShapeDtypeStruct((rows, 128), F32),
        (q_dec, k_grown, values),
        flops=2 * rows * rows * 512,
        moved=2 << 20,
        limit=12,
    )
    sent, before = call(
        spread_body,
        (packed_shape, jax.ShapeDtypeStruct((72, 384), F32)),
        (at, packed, *row),
        specs=[SMEM] + [VMEM] * 4,
        flops=64 * 384 * 30,
        moved=400 << 10,
    )
    above = [shifted(sent, "y", k) for k in (1, 2, 3)]
    half = jax.ShapeDtypeStruct((rows // 2, 128), BF16)
    keep, give = call(
        head_body,
        (half, half),
        (at, q_dec, before, *above, intra, gates, gain[None]),
        scratch=[pltpu.VMEM((rows, 128), F32)],
        specs=[SMEM] + [VMEM] * 8,
        flops=2 * 512 * 384 * 64,
        moved=1 << 20,
        limit=8,
    )
    return keep, partner(give), w_own


def project_body(at, keep, got, near, w0, w1, w2, w3, *refs):
    outs, rows = refs[:4], refs[4]
    shift = at[0]
    for i in range(4):
        here = slice(32 * i, 32 * i + 32)
        rows[here, :128] = keep[64 * i : 64 * i + 32, :]
        rows[here, 128:256] = got[64 * i : 64 * i + 32, :]
        there = pl.ds(pl.multiple_of(((i + shift) % 4) * 32, 32), 32)
        rows[here, 256:] = near[there, :]
    for tile in range(4):
        cols = slice(512 * tile, 512 * tile + 512)
        part = dot(rows[:, :128], w0[:, cols]) + dot(rows[:, 128:256], w1[:, cols])
        part = part + dot(rows[:, 256:384], w2[:, cols]) + dot(rows[:, 384:], w3[:, cols])
        part = part.astype(BF16)
        for i in range(4):
            outs[i][:, cols] = part[32 * i : 32 * i + 32]


def odd_blocks(v, size):
    return v.reshape(4, 2, size, v.shape[1])[:, 1].reshape(4 * size, v.shape[1])


def mixed_parts(keep, got, shift, w_own, w_other, w_near):
    near = neighbour(jnp.concatenate([odd_blocks(keep, 32), odd_blocks(got, 32)], axis=1))
    outs = call(
        project_body,
        tuple(jax.ShapeDtypeStruct((32, 2048), BF16) for _ in range(4)),
        (shift, keep, got, near, w_own, w_other, w_near, partner(w_near)),
        scratch=[pltpu.VMEM((128, 512), BF16)],
        specs=[SMEM] + [VMEM] * 7,
        flops=2 * 128 * 512 * 2048,
        moved=4 << 20,
        limit=10,
    )
    return from_stride(outs)


def normed_body(p0, p1, p2, p3, skip, post, pre, placing, mid, sent):
    mixed = p0[...].astype(F32) + p1[...].astype(F32) + p2[...].astype(F32) + p3[...].astype(F32)
    h = (skip[...].astype(F32) + rms_scale(mixed, post[...])).astype(BF16)
    mid[...] = h
    normed = rms_scale(h.astype(F32), pre[...]).astype(BF16)
    sent[...] = dot(placing[...], normed).astype(BF16)


def up_rows(xs, x, g0, g1, u0, u1, hidden):
    first = 0
    for ref in xs:
        x[first : first + ref.shape[0], :] = ref[...]
        first += ref.shape[0]
    rows = x[...]
    for i, (g, u) in enumerate(((g0, u0), (g1, u1))):
        gate = dot(rows, g[...])
        hidden[:, 256 * i : 256 * i + 256] = (jax.nn.silu(gate) * dot(rows, u[...])).astype(BF16)
    return rows


def odd_body(*refs):
    up_rows(refs[:4], refs[9], *refs[4:9])


def even_body(member, *refs):
    xs, disp, (weights, hidden, weight, x) = refs[:4], refs[4], (refs[5:9], *refs[9:])
    rows = up_rows(xs, x, *weights, hidden)
    scores = jax.nn.sigmoid(dot_t(rows, disp[...]))
    s0, s1 = scores[:, 0:1], scores[:, 1:2]
    mine = jnp.where(member[0] == 0, s0, s1) / (s0 + s1)
    weight[...] = jnp.broadcast_to(mine, weight.shape)


def down_body(at, keep, near, weight, *refs):
    downs, outs, rows = refs[:4], refs[4:8], refs[8]
    shift = at[0]
    for i in range(4):
        here = slice(48 * i, 48 * i + 48)
        rows[here, :512] = keep[here, :]
        rows[here, 512:] = near[pl.ds(pl.multiple_of(((i + shift) % 4) * 48, 16), 48), :]
    scale = weight[:, 0:1]
    for tile in range(4):
        cols = slice(512 * tile, 512 * tile + 512)
        part, first = 0.0, 0
        for d in downs:
            part = part + dot(rows[:, first : first + d.shape[0]], d[:, cols])
            first += d.shape[0]
        part = (part * scale).astype(BF16)
        for i in range(4):
            outs[i][:, cols] = part[48 * i : 48 * i + 48]


def total_body(p0, p1, p2, p3, out):
    total = p0[...].astype(F32) + p1[...].astype(F32) + p2[...].astype(F32) + p3[...].astype(F32)
    out[...] = total.astype(BF16)


def experts(chunk, dispatcher, shift, ups, downs):
    own, r1, r2, r3, far, l3, l2, l1 = ring_gather(chunk)
    hidden = jax.ShapeDtypeStruct((192, 512), BF16)
    give = call(
        odd_body,
        hidden,
        (r1, r3, l3, l1, *ups),
        scratch=[pltpu.VMEM((192, 2048), BF16)],
        flops=4 * 192 * 2048 * 512,
        moved=6 << 20,
        limit=12,
    )
    near = neighbour(give)
    keep, weight = call(
        even_body,
        (hidden, jax.ShapeDtypeStruct((192, 128), F32)),
        ((lax.axis_index("z") // 4)[None], own, r2, far, l2, dispatcher, *ups),
        scratch=[pltpu.VMEM((192, 2048), BF16)],
        specs=[SMEM] + [VMEM] * 9,
        flops=4 * 192 * 2048 * 512,
        moved=6 << 20,
        limit=12,
    )
    outs = call(
        down_body,
        tuple(jax.ShapeDtypeStruct((48, 2048), BF16) for _ in range(4)),
        (shift, keep, near, weight, *downs),
        scratch=[pltpu.VMEM((192, 1024), BF16)],
        specs=[SMEM] + [VMEM] * 7,
        flops=2 * 192 * 1024 * 2048,
        moved=6 << 20,
        limit=12,
    )
    return call(
        total_body,
        jax.ShapeDtypeStruct((48, 2048), BF16),
        from_stride(outs),
        flops=4 * 48 * 2048,
        moved=16 * 48 * 2048,
    )


def shards(
    qa, fa, gap_a, qb, fb, gap_b, values, gates, bias, gain, w_a, w_b, skip,
    post_gain, pre_gain, last_gain, dispatcher, switch, expansion, contraction, cluster,
):
    switch, expansion, contraction = switch[0], expansion[0], contraction[0]
    ups = (switch, partner(switch), expansion, partner(expansion))
    shift = jnp.where(lax.axis_index("z") % 2 == 0, 3, 0)[None]
    groups, capacity, count = 16, 3, skip.shape[0]
    r_of = lax.broadcasted_iota(jnp.int32, (count, count), 0)
    r_at = lax.broadcasted_iota(jnp.int32, (count, count), 1)
    same = (cluster[:, None] == cluster[None, :]) & (r_of < r_at)
    slot = cluster * capacity + jnp.sum(same.astype(jnp.int32), axis=0)
    placing = (
        slot[None, :] == lax.broadcasted_iota(jnp.int32, (groups * capacity, count), 0)
    ).astype(BF16)
    keep, got, w_own = heads_of(
        qa, fa, gap_a, qb, fb, gap_b, values, gates, bias, gain, w_a, w_b
    )
    parts = mixed_parts(keep, got, shift, w_own, partner(w_own), neighbour(w_own))
    near_rows = neighbour(contraction)
    h_mid, sent = call(
        normed_body,
        (jax.ShapeDtypeStruct((count, 2048), BF16), jax.ShapeDtypeStruct((48, 2048), BF16)),
        (*parts, skip, post_gain[None], pre_gain[None], placing),
        flops=2 * 48 * 32 * 2048,
        moved=1 << 20,
        limit=8,
    )
    chunk = lax.all_to_all(
        sent.reshape(groups, capacity, -1), ("y", "x"), 0, 0, tiled=True
    ).reshape(groups * capacity, -1)
    downs = (contraction, partner(contraction), near_rows, partner(near_rows))
    summed = experts(chunk, dispatcher.T, shift, ups, downs)
    back = lax.all_to_all(
        summed.reshape(groups, capacity, -1), ("y", "x"), 0, 0, tiled=True
    ).reshape(groups * capacity, -1)
    routed = dot_0(placing, back)
    return (h_mid.astype(F32) + rms_scale(routed, last_gain)).astype(BF16)


def solution(mesh):
    fine = Mesh(mesh.devices.reshape(4, 4, 8, 2), ("y", "x", "z", "core"))
    sp, tp = ("y", "x"), ("z", "core")
    both = sp + tp
    placed = (
        P(sp, tp), P(sp, tp), P(tp), P(sp, tp), P(sp, tp), P(tp), P(sp, tp), P(sp, tp), P(sp, tp),
        P(), P(tp, None), P(tp, None), P(both, None), P(), P(), P(), P(None, sp),
        P(sp, None, tp), P(sp, None, tp), P(sp, tp, None), P(both),
    )

    return jax.shard_map(
        shards, mesh=fine, in_specs=placed, out_specs=P(both, None), check_vma=False
    )
```

profile of v0, /device:TPU:32, one launch (start us, length us, event | category | flops | bytes accessed | tf_op | source)
XLA Modules:
  0.0 159.6 jit_solution(15690565842367635863)
XLA Ops:
  0.0 5.5 %shard_map.199 = (bf16[80,384]{1,0:T(8,128)(2,1)}, bf16[512,384]{1,0:T(8,128)(2,1)}, bf16[512,384]{1,0:T(8,128)(2,1)}, bf16[128,2048]{1,0:T(8,128)(2,1)}) custom-call(bf16[512,128]{1,0:T(8,128)(2,1)} %refs_0_.1, bf16[512,128]{1,0:T(8,128)(2,1)} %refs_1_.1, bf16[512,256]{1,0:T(8,128)(2,1)} %refs_2_.1, bf16[512,256]{1,0:T(8,128)(2,1)} %refs_3_.1, ...), custom_call_target="tpu_custom_call" | custom-call | flops 603979776 | bytes 3145728 | tf_op jit(solution)/shard_map/pallas_call | solution.py:45
  5.5 1.9 %collective-permute-start.9 = (bf16[128,2048]{1,0:T(8,128)(2,1)}, bf16[128,2048]{1,0:T(8,128)(2,1)}, u32[]{:S(2)}, u32[]{:S(2)}) collective-permute-start(bf16[128,2048]{1,0:T(8,128)(2,1)} %get-tuple-element.32.w0), channel_id=1, source_target_pairs={{0,2},{2,0},{4,6},{6,4},{8,10},{10,8},{12,14},{14,12},{1,3},{3,1},... | collective-permute-start | bytes 1572872 | tf_op jit(solution)/shard_map/ppermute | solution.py:57
  7.5 0.2 collective-permute-start.25
  7.7 1.5 collective-permute-start
  9.2 2.7 %collective-permute-start.1 = (bf16[80,384]{1,0:T(8,128)(2,1)}, bf16[80,384]{1,0:T(8,128)(2,1)S(1)}, u32[]{:S(2)}, u32[]{:S(2)}) collective-permute-start(bf16[80,384]{1,0:T(8,128)(2,1)} %get-tuple-element.26.own), channel_id=1, source_target_pairs={{0,32},{16,48},{32,0},{48,16},{1,33},{17,49},{33,1},{49,17},{2,34}... | collective-permute-start | bytes 184328 | tf_op jit(solution)/shard_map/ppermute | solution.py:19
  11.9 1.4 collective-permute-start.2
  13.3 0.6 collective-permute-done.got1
  13.9 6.8 %collective-permute-done.9.w2 = bf16[128,2048]{1,0:T(8,128)(2,1)} collective-permute-done((bf16[128,2048]{1,0:T(8,128)(2,1)}, bf16[128,2048]{1,0:T(8,128)(2,1)}, u32[]{:S(2)}, u32[]{:S(2)}) %collective-permute-start.9) | collective-permute-done | bytes 524320 | tf_op jit(solution)/shard_map/ppermute | solution.py:57
  20.8 0.8 copy-done.12
  21.7 0.7 shard_map.200
  22.4 1.7 %collective-permute-start.3 = (bf16[80,384]{1,0:T(8,128)(2,1)S(1)}, bf16[80,384]{1,0:T(8,128)(2,1)S(1)}, u32[]{:S(2)}, u32[]{:S(2)}) collective-permute-start(bf16[80,384]{1,0:T(8,128)(2,1)S(1)} %get-tuple-element.28), channel_id=1, source_target_pairs={{0,64},{64,128},{128,192},{192,0},{1,65},{65,129},{129,193},{193,1... | collective-permute-start | bytes 184328 | tf_op jit(solution)/shard_map/ppermute | solution.py:19
  24.0 2.9 %collective-permute-start.4 = (bf16[80,384]{1,0:T(8,128)(2,1)S(1)}, bf16[80,384]{1,0:T(8,128)(2,1)S(1)}, u32[]{:S(2)}, u32[]{:S(2)}) collective-permute-start(bf16[80,384]{1,0:T(8,128)(2,1)S(1)} %get-tuple-element.28), channel_id=1, source_target_pairs={{0,128},{64,192},{128,0},{192,64},{1,129},{65,193},{129,1},{193,65... | collective-permute-start | bytes 184328 | tf_op jit(solution)/shard_map/ppermute | solution.py:19
  26.9 1.2 collective-permute-done.3.got1
  28.1 2.5 %collective-permute-done.4.got2 = bf16[80,384]{1,0:T(8,128)(2,1)S(1)} collective-permute-done((bf16[80,384]{1,0:T(8,128)(2,1)S(1)}, bf16[80,384]{1,0:T(8,128)(2,1)S(1)}, u32[]{:S(2)}, u32[]{:S(2)}) %collective-permute-start.4) | collective-permute-done | bytes 61472 | tf_op jit(solution)/shard_map/ppermute | solution.py:19
  30.6 0.9 collective-permute-start.5
  31.5 1.0 copy-done.2
  32.5 1.0 copy-done.4
  33.5 0.9 shard_map.201.intra
  34.4 0.5 collective-permute-done.5.got3
  34.9 0.7 copy-done.16
  35.5 1.7 %shard_map.202 = (bf16[256,128]{1,0:T(8,128)(2,1)S(1)}, bf16[256,128]{1,0:T(8,128)(2,1)S(1)}) custom-call(s32[4]{0:T(128)S(1)} %pad_add_fusion.at, bf16[512,384]{1,0:T(8,128)(2,1)S(1)} %copy-done.2, f32[72,384]{1,0:T(8,128)S(1)} %get-tuple-element.27.before, bf16[80,384]{1,0:T(8,128)(2,1)S(1)} %collective-permute-done.3.got1, ...), custom_call_target="tpu_custom_call" | custom-call | flops 25165824 | bytes 1048576 | tf_op jit(solution)/shard_map/pallas_call | solution.py:45
  37.3 1.2 collective-permute-done.6.got
  38.6 1.4 collective-permute-start.7
  40.0 3.4 %collective-permute-done.7.near = bf16[128,256]{1,0:T(8,128)(2,1)S(1)} collective-permute-done((bf16[128,256]{1,0:T(8,128)(2,1)S(1)}, bf16[128,256]{1,0:T(8,128)(2,1)S(1)}, u32[]{:S(2)}, u32[]{:S(2)}) %collective-permute-start.7) | collective-permute-done | bytes 65568 | tf_op jit(solution)/shard_map/ppermute | solution.py:57
  43.4 1.0 copy-done.3
  44.4 2.1 %shard_map.203 = (bf16[32,2048]{1,0:T(8,128)(2,1)S(1)}, bf16[32,2048]{1,0:T(8,128)(2,1)S(1)}, bf16[32,2048]{1,0:T(8,128)(2,1)S(1)}, bf16[32,2048]{1,0:T(8,128)(2,1)S(1)}) custom-call(s32[1]{0:T(128)} %bitcast.at, bf16[256,128]{1,0:T(8,128)(2,1)S(1)} %get-tuple-element.30.keep, bf16[256,128]{1,0:T(8,128)(2,1)S(1)} %collective-permute-done.6.got, ...), custom_call_target="tpu_custom_call" | custom-call | flops 268435456 | bytes 4194304 | tf_op jit(solution)/shard_map/pallas_call | solution.py:45
  46.6 3.4 %collective-permute-start.11 = (bf16[32,2048]{1,0:T(8,128)(2,1)S(1)}, bf16[32,2048]{1,0:T(8,128)(2,1)S(1)}, u32[]{:S(2)}, u32[]{:S(2)}) collective-permute-start(bf16[32,2048]{1,0:T(8,128)(2,1)S(1)} %get-tuple-element.34), channel_id=1, source_target_pairs={{0,4},{2,6},{4,8},{6,10},{8,12},{10,14},{12,0},{14,2},{1,5},{3,7},... | collective-permute-start | bytes 393224 | tf_op jit(solution)/shard_map/ppermute | solution.py:19
  49.9 2.2 %collective-permute-start.12 = (bf16[32,2048]{1,0:T(8,128)(2,1)S(1)}, bf16[32,2048]{1,0:T(8,128)(2,1)S(1)}, u32[]{:S(2)}, u32[]{:S(2)}) collective-permute-start(bf16[32,2048]{1,0:T(8,128)(2,1)S(1)} %get-tuple-element.35), channel_id=1, source_target_pairs={{0,12},{2,14},{4,0},{6,2},{8,4},{10,6},{12,8},{14,10},{1,13},{3,15... | collective-permute-start | bytes 393224 | tf_op jit(solution)/shard_map/ppermute | solution.py:19
  52.1 0.2 collective-permute-start.24
  52.3 6.7 %collective-permute-done.11.p1 = bf16[32,2048]{1,0:T(8,128)(2,1)S(1)} collective-permute-done((bf16[32,2048]{1,0:T(8,128)(2,1)S(1)}, bf16[32,2048]{1,0:T(8,128)(2,1)S(1)}, u32[]{:S(2)}, u32[]{:S(2)}) %collective-permute-start.11) | collective-permute-done | bytes 131104 | tf_op jit(solution)/shard_map/ppermute | solution.py:19
  59.0 3.0 %collective-permute-start.13 = (bf16[32,2048]{1,0:T(8,128)(2,1)S(1)}, bf16[32,2048]{1,0:T(8,128)(2,1)S(1)}, u32[]{:S(2)}, u32[]{:S(2)}) collective-permute-start(bf16[32,2048]{1,0:T(8,128)(2,1)S(1)} %get-tuple-element.36), channel_id=1, source_target_pairs={{0,8},{2,10},{4,12},{6,14},{8,0},{10,2},{12,4},{14,6},{1,9},{3,11}... | collective-permute-start | bytes 393224 | tf_op jit(solution)/shard_map/ppermute | solution.py:19
  62.0 8.9 %collective-permute-done.13.p3 = bf16[32,2048]{1,0:T(8,128)(2,1)S(1)} collective-permute-done((bf16[32,2048]{1,0:T(8,128)(2,1)S(1)}, bf16[32,2048]{1,0:T(8,128)(2,1)S(1)}, u32[]{:S(2)}, u32[]{:S(2)}) %collective-permute-start.13) | collective-permute-done | bytes 131104 | tf_op jit(solution)/shard_map/ppermute | solution.py:19
  70.9 0.5 shard_map.204
  71.4 0.6 copy-done.9
  72.0 0.8 reshape.32
  72.9 16.0 %all_to_all.10 = bf16[16,3,2048]{2,1,0:T(4,128)(2,1)} all-to-all(bf16[16,3,2048]{2,1,0:T(4,128)(2,1)} %reshape.32), channel_id=1, replica_groups=mesh['y'=4,'x'=4,'z'=8,'core'=2] {'y','x'}, dimensions={0} | all-to-all | bytes 393216 | tf_op jit(solution)/shard_map/all_to_all | solution.py:387
  88.9 1.1 reshape.33.refs_0_
  90.1 2.0 %collective-permute-start.14 = (bf16[48,2048]{1,0:T(8,128)(2,1)S(1)}, bf16[48,2048]{1,0:T(8,128)(2,1)S(1)}, u32[]{:S(2)}, u32[]{:S(2)}) collective-permute-start(bf16[48,2048]{1,0:T(8,128)(2,1)S(1)} %reshape.33.refs_0_), channel_id=1, source_target_pairs={{0,14},{2,0},{4,2},{6,4},{8,6},{10,8},{12,10},{14,12},{1,15},{3,1}... | collective-permute-start | bytes 589832 | tf_op jit(solution)/shard_map/ppermute | solution.py:19
  92.1 3.7 %collective-permute-done.16.refs_3_ = bf16[48,2048]{1,0:T(8,128)(2,1)S(1)} collective-permute-done((bf16[48,2048]{1,0:T(8,128)(2,1)S(1)}, bf16[48,2048]{1,0:T(8,128)(2,1)S(1)}, u32[]{:S(2)}, u32[]{:S(2)}) %collective-permute-start.16) | collective-permute-done | bytes 196640 | tf_op jit(solution)/shard_map/ppermute | solution.py:19
  95.8 0.3 collective-permute-start.17
  96.1 1.7 %collective-permute-start.15 = (bf16[48,2048]{1,0:T(8,128)(2,1)S(1)}, bf16[48,2048]{1,0:T(8,128)(2,1)S(1)}, u32[]{:S(2)}, u32[]{:S(2)}) collective-permute-start(bf16[48,2048]{1,0:T(8,128)(2,1)S(1)} %collective-permute-done.14.refs_0_), channel_id=1, source_target_pairs={{0,14},{2,0},{4,2},{6,4},{8,6},{10,8},{12,10},{14,12},{1,15},{3,1}... | collective-permute-start | bytes 589832 | tf_op jit(solution)/shard_map/ppermute | solution.py:19
  97.8 4.2 %collective-permute-done.17.refs_3_ = bf16[48,2048]{1,0:T(8,128)(2,1)S(1)} collective-permute-done((bf16[48,2048]{1,0:T(8,128)(2,1)S(1)}, bf16[48,2048]{1,0:T(8,128)(2,1)S(1)}, u32[]{:S(2)}, u32[]{:S(2)}) %collective-permute-start.17) | collective-permute-done | bytes 196640 | tf_op jit(solution)/shard_map/ppermute | solution.py:19
  102.0 0.6 collective-permute-start.18
  102.6 0.5 collective-permute-done.15.refs_1_
  103.1 0.9 collective-permute-start.22
  104.0 0.7 copy-done.5
  104.7 4.4 %collective-permute-done.18.refs_2_ = bf16[48,2048]{1,0:T(8,128)(2,1)} collective-permute-done((bf16[48,2048]{1,0:T(8,128)(2,1)S(1)}, bf16[48,2048]{1,0:T(8,128)(2,1)}, u32[]{:S(2)}, u32[]{:S(2)}) %collective-permute-start.18) | collective-permute-done | bytes 196640 | tf_op jit(solution)/shard_map/ppermute | solution.py:19
  109.1 2.6 %collective-permute-start.19 = (bf16[48,2048]{1,0:T(8,128)(2,1)}, bf16[48,2048]{1,0:T(8,128)(2,1)}, u32[]{:S(2)}, u32[]{:S(2)}) collective-permute-start(bf16[48,2048]{1,0:T(8,128)(2,1)} %collective-permute-done.18.refs_2_), channel_id=1, source_target_pairs={{0,2},{2,4},{4,6},{6,8},{8,10},{10,12},{12,14},{14,0},{1,3},{3,5},... | collective-permute-start | bytes 589832 | tf_op jit(solution)/shard_map/ppermute | solution.py:19
  111.7 3.0 %shard_map.206 = bf16[192,512]{1,0:T(8,128)(2,1)} custom-call(bf16[48,2048]{1,0:T(8,128)(2,1)S(1)} %collective-permute-done.14.refs_0_, bf16[48,2048]{1,0:T(8,128)(2,1)S(1)} %collective-permute-done.22.refs_1_, bf16[48,2048]{1,0:T(8,128)(2,1)} %collective-permute-done.18.refs_2_, bf16[48,2048]{1,0:T(8,128)(2,1)S(1)} %collective-permute-done.16.refs_3_, ...), custom_call_target="tpu_custom_call" | custom-call | flops 805306368 | bytes 6291456 | tf_op jit(solution)/shard_map/pallas_call | solution.py:45
  114.7 0.5 collective-permute-done.19.refs_2_
  115.2 0.2 copy-done.15
  115.4 0.9 copy-done.6
  116.3 2.7 %shard_map.205 = (bf16[192,512]{1,0:T(8,128)(2,1)S(1)}, f32[192,128]{1,0:T(8,128)S(1)}) custom-call(s32[1]{0:T(128)} %bitcast.15.member, bf16[48,2048]{1,0:T(8,128)(2,1)S(1)} %reshape.33.refs_0_, bf16[48,2048]{1,0:T(8,128)(2,1)S(1)} %copy-done.6, bf16[48,2048]{1,0:T(8,128)(2,1)} %collective-permute-done.19.refs_2_, ...), custom_call_target="tpu_custom_call" | custom-call | flops 805306368 | bytes 6291456 | tf_op jit(solution)/shard_map/pallas_call | solution.py:45
  119.0 1.7 %collective-permute-done.23.near = bf16[192,512]{1,0:T(8,128)(2,1)} collective-permute-done((bf16[192,512]{1,0:T(8,128)(2,1)}, bf16[192,512]{1,0:T(8,128)(2,1)}, u32[]{:S(2)}, u32[]{:S(2)}) %collective-permute-start.23) | collective-permute-done | bytes 196640 | tf_op jit(solution)/shard_map/ppermute | solution.py:57
  120.7 3.2 %shard_map.207 = (bf16[48,2048]{1,0:T(8,128)(2,1)S(1)}, bf16[48,2048]{1,0:T(8,128)(2,1)S(1)}, bf16[48,2048]{1,0:T(8,128)(2,1)S(1)}, bf16[48,2048]{1,0:T(8,128)(2,1)S(1)}) custom-call(s32[1]{0:T(128)} %bitcast.at, bf16[192,512]{1,0:T(8,128)(2,1)S(1)} %get-tuple-element.39.keep, bf16[192,512]{1,0:T(8,128)(2,1)} %collective-permute-done.23.near, ...), custom_call_target="tpu_custom_call" | custom-call | flops 805306368 | bytes 6291456 | tf_op jit(solution)/shard_map/pallas_call | solution.py:45
  123.9 9.7 %collective-permute-start.27 = (bf16[48,2048]{1,0:T(8,128)(2,1)S(1)}, bf16[48,2048]{1,0:T(8,128)(2,1)S(1)}, u32[]{:S(2)}, u32[]{:S(2)}) collective-permute-start(bf16[48,2048]{1,0:T(8,128)(2,1)S(1)} %get-tuple-element.42), channel_id=1, source_target_pairs={{0,4},{2,6},{4,8},{6,10},{8,12},{10,14},{12,0},{14,2},{1,5},{3,7},... | collective-permute-start | bytes 589832 | tf_op jit(solution)/shard_map/ppermute | solution.py:19
  133.6 3.7 %collective-permute-start.29 = (bf16[48,2048]{1,0:T(8,128)(2,1)S(1)}, bf16[48,2048]{1,0:T(8,128)(2,1)S(1)}, u32[]{:S(2)}, u32[]{:S(2)}) collective-permute-start(bf16[48,2048]{1,0:T(8,128)(2,1)S(1)} %get-tuple-element.44), channel_id=1, source_target_pairs={{0,8},{2,10},{4,12},{6,14},{8,0},{10,2},{12,4},{14,6},{1,9},{3,11}... | collective-permute-start | bytes 589832 | tf_op jit(solution)/shard_map/ppermute | solution.py:19
  137.3 6.2 %collective-permute-done.27.p1 = bf16[48,2048]{1,0:T(8,128)(2,1)S(1)} collective-permute-done((bf16[48,2048]{1,0:T(8,128)(2,1)S(1)}, bf16[48,2048]{1,0:T(8,128)(2,1)S(1)}, u32[]{:S(2)}, u32[]{:S(2)}) %collective-permute-start.27) | collective-permute-done | bytes 196640 | tf_op jit(solution)/shard_map/ppermute | solution.py:19
  143.5 2.6 %collective-permute-done.29.p3 = bf16[48,2048]{1,0:T(8,128)(2,1)S(1)} collective-permute-done((bf16[48,2048]{1,0:T(8,128)(2,1)S(1)}, bf16[48,2048]{1,0:T(8,128)(2,1)S(1)}, u32[]{:S(2)}, u32[]{:S(2)}) %collective-permute-start.29) | collective-permute-done | bytes 196640 | tf_op jit(solution)/shard_map/ppermute | solution.py:19
  146.3 11.4 %all_to_all.11 = bf16[16,3,2048]{2,1,0:T(4,128)(2,1)S(1)} all-to-all(bf16[16,3,2048]{2,1,0:T(4,128)(2,1)S(1)} %reshape.34), channel_id=1, replica_groups=mesh['y'=4,'x'=4,'z'=8,'core'=2] {'y','x'}, dimensions={0} | all-to-all | bytes 393216 | tf_op jit(solution)/shard_map/all_to_all | solution.py:392
  157.7 0.2 reshape.35
  157.9 0.3 multiply_reduce_fusion
  158.3 0.5 copy-done.10
  158.8 0.8 add_convert_fusion
  (60 shorter events, 0.7 us)
Async XLA Ops:
  0.0 28.1 %copy-start = (bf16[1,2048,256]{2,1,0:T(8,128)(2,1)S(1)}, bf16[1,2048,256]{2,1,0:T(8,128)(2,1)}, u32[]{:S(2)}) copy-start(bf16[1,2048,256]{2,1,0:T(8,128)(2,1)} %param.38) | copy-start | bytes 3145732
  5.5 15.2 %collective-permute-start.9 = (bf16[128,2048]{1,0:T(8,128)(2,1)}, bf16[128,2048]{1,0:T(8,128)(2,1)}, u32[]{:S(2)}, u32[]{:S(2)}) collective-permute-start(bf16[128,2048]{1,0:T(8,128)(2,1)} %get-tuple-element.32.w0), channel_id=1, source_target_pairs={{0,2},{2,0},{4,6},{6,4},{8,10},{10,8},{12,14},{14,12},{1,3},{3,1},... | collective-permute-start | bytes 1572872 | tf_op jit(solution)/shard_map/ppermute | solution.py:57
  7.5 44.7 %collective-permute-start.25 = (bf16[256,2048]{1,0:T(8,128)(2,1)}, bf16[256,2048]{1,0:T(8,128)(2,1)}, u32[]{:S(2)}, u32[]{:S(2)}) collective-permute-start(bf16[256,2048]{1,0:T(8,128)(2,1)} %bitcast.19.refs_0_), channel_id=1, source_target_pairs={{0,2},{2,0},{4,6},{6,4},{8,10},{10,8},{12,14},{14,12},{1,3},{3,1},... | collective-permute-start | bytes 3145736 | tf_op jit(solution)/shard_map/ppermute | solution.py:57
  7.7 6.2 %collective-permute-start = (bf16[80,384]{1,0:T(8,128)(2,1)}, bf16[80,384]{1,0:T(8,128)(2,1)S(1)}, u32[]{:S(2)}, u32[]{:S(2)}) collective-permute-start(bf16[80,384]{1,0:T(8,128)(2,1)} %get-tuple-element.26.own), channel_id=1, source_target_pairs={{0,16},{16,32},{32,48},{48,0},{1,17},{17,33},{33,49},{49,1},{2,18}... | collective-permute-start | bytes 184328 | tf_op jit(solution)/shard_map/ppermute | solution.py:19
  9.2 11.7 %collective-permute-start.1 = (bf16[80,384]{1,0:T(8,128)(2,1)}, bf16[80,384]{1,0:T(8,128)(2,1)S(1)}, u32[]{:S(2)}, u32[]{:S(2)}) collective-permute-start(bf16[80,384]{1,0:T(8,128)(2,1)} %get-tuple-element.26.own), channel_id=1, source_target_pairs={{0,32},{16,48},{32,0},{48,16},{1,33},{17,49},{33,1},{49,17},{2,34}... | collective-permute-start | bytes 184328 | tf_op jit(solution)/shard_map/ppermute | solution.py:19
  11.9 9.0 %collective-permute-start.2 = (bf16[80,384]{1,0:T(8,128)(2,1)}, bf16[80,384]{1,0:T(8,128)(2,1)S(1)}, u32[]{:S(2)}, u32[]{:S(2)}) collective-permute-start(bf16[80,384]{1,0:T(8,128)(2,1)} %get-tuple-element.26.own), channel_id=1, source_target_pairs={{0,48},{16,0},{32,16},{48,32},{1,49},{17,1},{33,17},{49,33},{2,50}... | collective-permute-start | bytes 184328 | tf_op jit(solution)/shard_map/ppermute | solution.py:19
  13.9 29.5 %collective-permute-start.8 = (bf16[128,2048]{1,0:T(8,128)(2,1)}, bf16[128,2048]{1,0:T(8,128)(2,1)}, u32[]{:S(2)}, u32[]{:S(2)}) collective-permute-start(bf16[128,2048]{1,0:T(8,128)(2,1)} %get-tuple-element.32.w0), channel_id=1, source_target_pairs={{0,1},{1,0},{2,3},{3,2},{4,5},{5,4},{6,7},{7,6},{8,9},{9,8},{10,11... | collective-permute-start | bytes 1572872 | tf_op jit(solution)/shard_map/ppermute | solution.py:23
  20.7 22.6 %collective-permute-start.10 = (bf16[128,2048]{1,0:T(8,128)(2,1)}, bf16[128,2048]{1,0:T(8,128)(2,1)}, u32[]{:S(2)}, u32[]{:S(2)}) collective-permute-start(bf16[128,2048]{1,0:T(8,128)(2,1)} %collective-permute-done.9.w2), channel_id=1, source_target_pairs={{0,1},{1,0},{2,3},{3,2},{4,5},{5,4},{6,7},{7,6},{8,9},{9,8},{10,11... | collective-permute-start | bytes 1572872 | tf_op jit(solution)/shard_map/ppermute | solution.py:23
  20.7 10.7 %copy-start.7 = (bf16[512,128]{1,0:T(8,128)(2,1)S(1)}, bf16[512,128]{1,0:T(8,128)(2,1)}, u32[]{:S(2)}) copy-start(bf16[512,128]{1,0:T(8,128)(2,1)} %values.1) | copy-start | bytes 393220
  20.8 0.8 copy-start.12
  22.4 5.8 %collective-permute-start.3 = (bf16[80,384]{1,0:T(8,128)(2,1)S(1)}, bf16[80,384]{1,0:T(8,128)(2,1)S(1)}, u32[]{:S(2)}, u32[]{:S(2)}) collective-permute-start(bf16[80,384]{1,0:T(8,128)(2,1)S(1)} %get-tuple-element.28), channel_id=1, source_target_pairs={{0,64},{64,128},{128,192},{192,0},{1,65},{65,129},{129,193},{193,1... | collective-permute-start | bytes 184328 | tf_op jit(solution)/shard_map/ppermute | solution.py:19
  24.0 6.6 %collective-permute-start.4 = (bf16[80,384]{1,0:T(8,128)(2,1)S(1)}, bf16[80,384]{1,0:T(8,128)(2,1)S(1)}, u32[]{:S(2)}, u32[]{:S(2)}) collective-permute-start(bf16[80,384]{1,0:T(8,128)(2,1)S(1)} %get-tuple-element.28), channel_id=1, source_target_pairs={{0,128},{64,192},{128,0},{192,64},{1,129},{65,193},{129,1},{193,65... | collective-permute-start | bytes 184328 | tf_op jit(solution)/shard_map/ppermute | solution.py:19
  28.1 62.0 %collective-permute-start.20 = (bf16[2048,256]{1,0:T(8,128)(2,1)S(1)}, bf16[2048,256]{1,0:T(8,128)(2,1)S(1)}, u32[]{:S(2)}, u32[]{:S(2)}) collective-permute-start(bf16[2048,256]{1,0:T(8,128)(2,1)S(1)} %bitcast.25), channel_id=1, source_target_pairs={{0,1},{1,0},{2,3},{3,2},{4,5},{5,4},{6,7},{7,6},{8,9},{9,8},{10,11... | collective-permute-start | bytes 3145736 | tf_op jit(solution)/shard_map/ppermute | solution.py:23
  30.6 4.2 %collective-permute-start.5 = (bf16[80,384]{1,0:T(8,128)(2,1)S(1)}, bf16[80,384]{1,0:T(8,128)(2,1)S(1)}, u32[]{:S(2)}, u32[]{:S(2)}) collective-permute-start(bf16[80,384]{1,0:T(8,128)(2,1)S(1)} %get-tuple-element.28), channel_id=1, source_target_pairs={{0,192},{64,0},{128,64},{192,128},{1,193},{65,1},{129,65},{193,129... | collective-permute-start | bytes 184328 | tf_op jit(solution)/shard_map/ppermute | solution.py:19
  31.5 1.0 copy-start.2
  32.5 1.0 copy-start.4
  33.5 1.4 copy-start.8
  33.5 9.9 %copy-start.1 = (bf16[1,2048,256]{2,1,0:T(8,128)(2,1)S(1)}, bf16[1,2048,256]{2,1,0:T(8,128)(2,1)}, u32[]{:S(2)}) copy-start(bf16[1,2048,256]{2,1,0:T(8,128)(2,1)} %param.39) | copy-start | bytes 3145732
  34.9 0.7 copy-start.16
  37.2 1.3 collective-permute-start.6
  38.6 1.4 copy-start.18
  38.6 4.8 %collective-permute-start.7 = (bf16[128,256]{1,0:T(8,128)(2,1)S(1)}, bf16[128,256]{1,0:T(8,128)(2,1)S(1)}, u32[]{:S(2)}, u32[]{:S(2)}) collective-permute-start(bf16[128,256]{1,0:T(8,128)(2,1)S(1)} %pad_maximum_fusion), channel_id=1, source_target_pairs={{0,2},{2,0},{4,6},{6,4},{8,10},{10,8},{12,14},{14,12},{1,3},{3,1},... | collective-permute-start | bytes 196616 | tf_op jit(solution)/shard_map/ppermute | solution.py:57
  43.4 68.3 %collective-permute-start.21 = (bf16[2048,256]{1,0:T(8,128)(2,1)S(1)}, bf16[2048,256]{1,0:T(8,128)(2,1)}, u32[]{:S(2)}, u32[]{:S(2)}) collective-permute-start(bf16[2048,256]{1,0:T(8,128)(2,1)S(1)} %bitcast.28), channel_id=1, source_target_pairs={{0,1},{1,0},{2,3},{3,2},{4,5},{5,4},{6,7},{7,6},{8,9},{9,8},{10,11... | collective-permute-start | bytes 3145736 | tf_op jit(solution)/shard_map/ppermute | solution.py:23
  43.4 1.0 copy-start.3
  44.4 26.5 %copy-start.11 = (bf16[32,2048]{1,0:T(8,128)(2,1)S(1)}, bf16[32,2048]{1,0:T(8,128)(2,1)}, u32[]{:S(2)}) copy-start(bf16[32,2048]{1,0:T(8,128)(2,1)} %skip.1) | copy-start | bytes 393220
  46.6 12.4 %collective-permute-start.11 = (bf16[32,2048]{1,0:T(8,128)(2,1)S(1)}, bf16[32,2048]{1,0:T(8,128)(2,1)S(1)}, u32[]{:S(2)}, u32[]{:S(2)}) collective-permute-start(bf16[32,2048]{1,0:T(8,128)(2,1)S(1)} %get-tuple-element.34), channel_id=1, source_target_pairs={{0,4},{2,6},{4,8},{6,10},{8,12},{10,14},{12,0},{14,2},{1,5},{3,7},... | collective-permute-start | bytes 393224 | tf_op jit(solution)/shard_map/ppermute | solution.py:19
  49.9 12.1 %collective-permute-start.12 = (bf16[32,2048]{1,0:T(8,128)(2,1)S(1)}, bf16[32,2048]{1,0:T(8,128)(2,1)S(1)}, u32[]{:S(2)}, u32[]{:S(2)}) collective-permute-start(bf16[32,2048]{1,0:T(8,128)(2,1)S(1)} %get-tuple-element.35), channel_id=1, source_target_pairs={{0,12},{2,14},{4,0},{6,2},{8,4},{10,6},{12,8},{14,10},{1,13},{3,15... | collective-permute-start | bytes 393224 | tf_op jit(solution)/shard_map/ppermute | solution.py:19
  52.1 66.8 %collective-permute-start.24 = (bf16[256,2048]{1,0:T(8,128)(2,1)}, bf16[256,2048]{1,0:T(8,128)(2,1)}, u32[]{:S(2)}, u32[]{:S(2)}) collective-permute-start(bf16[256,2048]{1,0:T(8,128)(2,1)} %bitcast.19.refs_0_), channel_id=1, source_target_pairs={{0,1},{1,0},{2,3},{3,2},{4,5},{5,4},{6,7},{7,6},{8,9},{9,8},{10,11... | collective-permute-start | bytes 3145736 | tf_op jit(solution)/shard_map/ppermute | solution.py:23
  59.0 11.9 %copy-start.13 = (f32[2048]{0:T(1024)S(1)}, f32[2048]{0:T(1024)}, u32[]{:S(2)}) copy-start(f32[2048]{0:T(1024)} %param.34) | copy-start | bytes 24580
  59.0 11.9 %copy-start.14 = (f32[2048]{0:T(1024)S(1)}, f32[2048]{0:T(1024)}, u32[]{:S(2)}) copy-start(f32[2048]{0:T(1024)} %param.35) | copy-start | bytes 24580
  59.0 11.9 %collective-permute-start.13 = (bf16[32,2048]{1,0:T(8,128)(2,1)S(1)}, bf16[32,2048]{1,0:T(8,128)(2,1)S(1)}, u32[]{:S(2)}, u32[]{:S(2)}) collective-permute-start(bf16[32,2048]{1,0:T(8,128)(2,1)S(1)} %get-tuple-element.36), channel_id=1, source_target_pairs={{0,8},{2,10},{4,12},{6,14},{8,0},{10,2},{12,4},{14,6},{1,9},{3,11}... | collective-permute-start | bytes 393224 | tf_op jit(solution)/shard_map/ppermute | solution.py:19
  62.0 57.0 %collective-permute-start.26 = (bf16[256,2048]{1,0:T(8,128)(2,1)}, bf16[256,2048]{1,0:T(8,128)(2,1)}, u32[]{:S(2)}, u32[]{:S(2)}) collective-permute-start(bf16[256,2048]{1,0:T(8,128)(2,1)} %collective-permute-done.25.refs_2_), channel_id=1, source_target_pairs={{0,1},{1,0},{2,3},{3,2},{4,5},{5,4},{6,7},{7,6},{8,9},{9,8},{10,11... | collective-permute-start | bytes 3145736 | tf_op jit(solution)/shard_map/ppermute | solution.py:23
  71.4 0.7 copy-start.9
  90.0 5.8 %collective-permute-start.16 = (bf16[48,2048]{1,0:T(8,128)(2,1)S(1)}, bf16[48,2048]{1,0:T(8,128)(2,1)S(1)}, u32[]{:S(2)}, u32[]{:S(2)}) collective-permute-start(bf16[48,2048]{1,0:T(8,128)(2,1)S(1)} %reshape.33.refs_0_), channel_id=1, source_target_pairs={{0,2},{2,4},{4,6},{6,8},{8,10},{10,12},{12,14},{14,0},{1,3},{3,5},... | collective-permute-start | bytes 589832 | tf_op jit(solution)/shard_map/ppermute | solution.py:19
  90.1 5.9 %collective-permute-start.14 = (bf16[48,2048]{1,0:T(8,128)(2,1)S(1)}, bf16[48,2048]{1,0:T(8,128)(2,1)S(1)}, u32[]{:S(2)}, u32[]{:S(2)}) collective-permute-start(bf16[48,2048]{1,0:T(8,128)(2,1)S(1)} %reshape.33.refs_0_), channel_id=1, source_target_pairs={{0,14},{2,0},{4,2},{6,4},{8,6},{10,8},{12,10},{14,12},{1,15},{3,1}... | collective-permute-start | bytes 589832 | tf_op jit(solution)/shard_map/ppermute | solution.py:19
  95.8 6.2 %collective-permute-start.17 = (bf16[48,2048]{1,0:T(8,128)(2,1)S(1)}, bf16[48,2048]{1,0:T(8,128)(2,1)S(1)}, u32[]{:S(2)}, u32[]{:S(2)}) collective-permute-start(bf16[48,2048]{1,0:T(8,128)(2,1)S(1)} %collective-permute-done.16.refs_3_), channel_id=1, source_target_pairs={{0,2},{2,4},{4,6},{6,8},{8,10},{10,12},{12,14},{14,0},{1,3},{3,5},... | collective-permute-start | bytes 589832 | tf_op jit(solution)/shard_map/ppermute | solution.py:19
  96.1 7.0 %collective-permute-start.15 = (bf16[48,2048]{1,0:T(8,128)(2,1)S(1)}, bf16[48,2048]{1,0:T(8,128)(2,1)S(1)}, u32[]{:S(2)}, u32[]{:S(2)}) collective-permute-start(bf16[48,2048]{1,0:T(8,128)(2,1)S(1)} %collective-permute-done.14.refs_0_), channel_id=1, source_target_pairs={{0,14},{2,0},{4,2},{6,4},{8,6},{10,8},{12,10},{14,12},{1,15},{3,1}... | collective-permute-start | bytes 589832 | tf_op jit(solution)/shard_map/ppermute | solution.py:19
  102.0 7.1 %collective-permute-start.18 = (bf16[48,2048]{1,0:T(8,128)(2,1)S(1)}, bf16[48,2048]{1,0:T(8,128)(2,1)}, u32[]{:S(2)}, u32[]{:S(2)}) collective-permute-start(bf16[48,2048]{1,0:T(8,128)(2,1)S(1)} %collective-permute-done.17.refs_3_), channel_id=1, source_target_pairs={{0,2},{2,4},{4,6},{6,8},{8,10},{10,12},{12,14},{14,0},{1,3},{3,5},... | collective-permute-start | bytes 589832 | tf_op jit(solution)/shard_map/ppermute | solution.py:19
  103.1 8.6 %collective-permute-start.22 = (bf16[48,2048]{1,0:T(8,128)(2,1)S(1)}, bf16[48,2048]{1,0:T(8,128)(2,1)S(1)}, u32[]{:S(2)}, u32[]{:S(2)}) collective-permute-start(bf16[48,2048]{1,0:T(8,128)(2,1)S(1)} %collective-permute-done.15.refs_1_), channel_id=1, source_target_pairs={{0,14},{2,0},{4,2},{6,4},{8,6},{10,8},{12,10},{14,12},{1,15},{3,1}... | collective-permute-start | bytes 589832 | tf_op jit(solution)/shard_map/ppermute | solution.py:19
  104.0 0.7 copy-start.5
  109.1 6.1 %collective-permute-start.19 = (bf16[48,2048]{1,0:T(8,128)(2,1)}, bf16[48,2048]{1,0:T(8,128)(2,1)}, u32[]{:S(2)}, u32[]{:S(2)}) collective-permute-start(bf16[48,2048]{1,0:T(8,128)(2,1)} %collective-permute-done.18.refs_2_), channel_id=1, source_target_pairs={{0,2},{2,4},{4,6},{6,8},{8,10},{10,12},{12,14},{14,0},{1,3},{3,5},... | collective-permute-start | bytes 589832 | tf_op jit(solution)/shard_map/ppermute | solution.py:19
  114.7 6.0 %collective-permute-start.23 = (bf16[192,512]{1,0:T(8,128)(2,1)}, bf16[192,512]{1,0:T(8,128)(2,1)}, u32[]{:S(2)}, u32[]{:S(2)}) collective-permute-start(bf16[192,512]{1,0:T(8,128)(2,1)} %shard_map.206), channel_id=1, source_target_pairs={{0,2},{2,0},{4,6},{6,4},{8,10},{10,8},{12,14},{14,12},{1,3},{3,1},... | collective-permute-start | bytes 589832 | tf_op jit(solution)/shard_map/ppermute | solution.py:57
  114.7 0.7 copy-start.15
  115.4 0.9 copy-start.6
  123.9 19.6 %collective-permute-start.27 = (bf16[48,2048]{1,0:T(8,128)(2,1)S(1)}, bf16[48,2048]{1,0:T(8,128)(2,1)S(1)}, u32[]{:S(2)}, u32[]{:S(2)}) collective-permute-start(bf16[48,2048]{1,0:T(8,128)(2,1)S(1)} %get-tuple-element.42), channel_id=1, source_target_pairs={{0,4},{2,6},{4,8},{6,10},{8,12},{10,14},{12,0},{14,2},{1,5},{3,7},... | collective-permute-start | bytes 589832 | tf_op jit(solution)/shard_map/ppermute | solution.py:19
  133.6 9.9 %collective-permute-start.28 = (bf16[48,2048]{1,0:T(8,128)(2,1)S(1)}, bf16[48,2048]{1,0:T(8,128)(2,1)S(1)}, u32[]{:S(2)}, u32[]{:S(2)}) collective-permute-start(bf16[48,2048]{1,0:T(8,128)(2,1)S(1)} %get-tuple-element.43), channel_id=1, source_target_pairs={{0,12},{2,14},{4,0},{6,2},{8,4},{10,6},{12,8},{14,10},{1,13},{3,15... | collective-permute-start | bytes 589832 | tf_op jit(solution)/shard_map/ppermute | solution.py:19
  133.6 12.5 %collective-permute-start.29 = (bf16[48,2048]{1,0:T(8,128)(2,1)S(1)}, bf16[48,2048]{1,0:T(8,128)(2,1)S(1)}, u32[]{:S(2)}, u32[]{:S(2)}) collective-permute-start(bf16[48,2048]{1,0:T(8,128)(2,1)S(1)} %get-tuple-element.44), channel_id=1, source_target_pairs={{0,8},{2,10},{4,12},{6,14},{8,0},{10,2},{12,4},{14,6},{1,9},{3,11}... | collective-permute-start | bytes 589832 | tf_op jit(solution)/shard_map/ppermute | solution.py:19
  157.9 0.9 copy-start.10
  157.9 0.9 copy-start.17
where the time goes:
time: 160 us
  waiting for transfers between devices  55.5 us (35%)
  starting transfers between devices  45 us (28%)
  blocking collectives  27.4 us (17%)
  Pallas kernels  20.4 us (13%)
  local copies, waits for them, and re-layouts  9.8 us (6%)
    ppermute x19, waiting for transfers between devices, shifted(): return lax.ppermute(v, axis, [(i, (i + by) % n) for i in range(n)])  42.4 us
    ppermute x19, starting transfers between devices, shifted(): return lax.ppermute(v, axis, [(i, (i + by) % n) for i in range(n)])  41.2 us
    pallas_call x10, Pallas kernels, call(): pl.pallas_call(body, out_shape=outs, in_specs=specs or [VMEM] * len(args)...  20.4 us
    all_to_all x1, blocking collectives, shards(): lax.all_to_all(sent.reshape(groups, capacity, -1), ('y', 'x'), 0, 0, tile...  16 us
    ppermute x4, waiting for transfers between devices, neighbour(): return lax.ppermute(v, 'z', [(i, i ^ 1) for i in range(8)])  11.9 us
    all_to_all x1, blocking collectives, shards(): lax.all_to_all(summed.reshape(groups, capacity, -1), ('y', 'x'), 0, 0, ti...  11.4 us
    unnamed x38, local copies, waits for them, and re-layouts  7.55 us
    ppermute x4, starting transfers between devices, neighbour(): return lax.ppermute(v, 'z', [(i, i ^ 1) for i in range(8)])  3.47 us
  transfers between devices with their start and end apart: 30, of which 17 were waited for; matrix products, arithmetic and copies ran while one was open for 1% of the time, Pallas kernels for 7%

commit v1 on v0

--- a/solution.py
+++ b/solution.py
@@ -100,7 +100,7 @@
 
 def prepare_body(*refs):
     far, (ga, gb, bias), refs = refs[:7], refs[7:10], refs[10:]
-    packed, q_dec, k_grown, weights, qa, fa, qb, fb, values, sems = refs
+    packed, both, weights, qa, fa, qb, fb, values, sems = refs
     near = (qa, fa, qb, fb, values, weights.at[:64], weights.at[64:])
     copies = [
         pltpu.make_async_copy(src, dst, sems.at[i]) for i, (src, dst) in enumerate(zip(far, near))
@@ -128,19 +128,19 @@
         k_last = (key * jnp.exp(total - inside)).astype(BF16)
         pack(packed, lanes, dot(flipped[64 * side : 64 * side + 64], k_last), total)
         copies[2 * side].wait()
-        q_dec[:, lanes] = (jax.nn.silu(q[...].astype(F32)) * jnp.exp(inside)).astype(BF16)
-        k_grown[:, lanes] = (key * jnp.exp(-inside)).astype(BF16)
+        both[:rows, lanes] = (jax.nn.silu(q[...].astype(F32)) * jnp.exp(inside)).astype(BF16)
+        both[rows:, lanes] = (key * jnp.exp(-inside)).astype(BF16)
     copies[5].wait()
     copies[6].wait()
 
 
-def inner_body(q_dec, k_grown, values, intra):
-    rows = q_dec.shape[0]
+def inner_body(both, values, intra):
+    rows = values.shape[0]
     at = lax.broadcasted_iota(jnp.int32, (rows, rows), 0)
     of = lax.broadcasted_iota(jnp.int32, (rows, rows), 1)
     for side, lanes in enumerate(SIDES):
         cols = slice(64 * side, 64 * side + 64)
-        scores = jnp.where(at >= of, dot_t(q_dec[:, lanes], k_grown[:, lanes]), 0.0).astype(BF16)
+        scores = jnp.where(at >= of, dot_t(both[:rows, lanes], both[rows:, lanes]), 0.0).astype(BF16)
         intra[:, cols] = dot(scores, values[:, cols])
 
 
@@ -154,14 +154,14 @@
     before[64:, :] = jnp.broadcast_to(total, (8, total.shape[1]))
 
 
-def head_body(at, q_dec, before, got1, got2, got3, intra, gates, gain, keep, give, heads):
+def head_body(at, both, before, got1, got2, got3, intra, gates, gain, keep, give, heads):
     y = at[3]
     rows_above = [unpack(ref) for ref in (got1, got2, got3)]
     above, _ = prefix_of(rows_above, [(y + 4 - k) % 4 for k in (1, 2, 3)], y)
     carried = (jnp.exp(before[64:65, :]) * above + before[:64, :]).astype(BF16)
     for side, lanes in enumerate(SIDES):
         cols = slice(64 * side, 64 * side + 64)
-        raw = intra[:, cols] + dot_t(q_dec[:, lanes], carried[:, lanes])
+        raw = intra[:, cols] + dot_t(both[:512, lanes], carried[:, lanes])
         gate = jax.nn.sigmoid(gates[:, cols].astype(F32))
         heads[:, cols] = rms_scale(raw, gain[...]) * gate
     z, core = at[1], at[2]
@@ -175,11 +175,11 @@
 def heads_of(qa, fa, gap_a, qb, fb, gap_b, values, gates, bias, gain, w_a, w_b):
     rows = qa.shape[0]
     packed_shape = jax.ShapeDtypeStruct((80, 384), BF16)
-    wide = jax.ShapeDtypeStruct((rows, 384), BF16)
+    wide = jax.ShapeDtypeStruct((2 * rows, 384), BF16)
     far = (qa, fa, qb, fb, values, w_a, w_b)
-    packed, q_dec, k_grown, w_own = call(
+    packed, both, w_own = call(
         prepare_body,
-        (packed_shape, wide, wide, jax.ShapeDtypeStruct((128, 2048), BF16)),
+        (packed_shape, wide, jax.ShapeDtypeStruct((128, 2048), BF16)),
         (*far, gap_a[None], gap_b[None], bias.T),
         scratch=[*(pltpu.VMEM(v.shape, BF16) for v in far[:5]), pltpu.SemaphoreType.DMA((7,))],
         specs=[HBM] * 7 + [VMEM] * 3,
@@ -192,7 +192,7 @@
     intra = call(
         inner_body,
         jax.ShapeDtypeStruct((rows, 128), F32),
-        (q_dec, k_grown, values),
+        (both, values),
         flops=2 * rows * rows * 512,
         moved=2 << 20,
         limit=12,
@@ -210,7 +210,7 @@
     keep, give = call(
         head_body,
         (half, half),
-        (at, q_dec, before, *above, intra, gates, gain[None]),
+        (at, both, before, *above, intra, gates, gain[None]),
         scratch=[pltpu.VMEM((rows, 128), F32)],
         specs=[SMEM] + [VMEM] * 8,
         flops=2 * 512 * 384 * 64,
@@ -266,10 +266,8 @@
 
 
 def up_rows(xs, x, g0, g1, u0, u1, hidden):
-    first = 0
-    for ref in xs:
-        x[first : first + ref.shape[0], :] = ref[...]
-        first += ref.shape[0]
+    for i, (ref, first) in enumerate(xs):
+        x[48 * i : 48 * i + 48, :] = ref[first : first + 48, :]
     rows = x[...]
     for i, (g, u) in enumerate(((g0, u0), (g1, u1))):
         gate = dot(rows, g[...])
@@ -278,35 +276,39 @@
 
 
 def odd_body(*refs):
-    up_rows(refs[:4], refs[9], *refs[4:9])
+    odd, even, ups, (hidden, early, x) = refs[:4], refs[4:7], refs[7:11], refs[11:]
+    for i, ref in enumerate(even):
+        early[48 * i : 48 * i + 48, :] = ref[...]
+    up_rows([(odd[i], 0) for i in range(4)], x, *ups, hidden)
 
 
 def even_body(member, *refs):
-    xs, disp, (weights, hidden, weight, x) = refs[:4], refs[4], (refs[5:9], *refs[9:])
-    rows = up_rows(xs, x, *weights, hidden)
+    early, far, disp, ups, downs = refs[0], refs[1], refs[2], refs[3:7], refs[7:9]
+    part, weight, x, hidden = refs[9:]
+    rows = up_rows([(early, 0), (early, 48), (far, 0), (early, 96)], x, *ups, hidden)
     scores = jax.nn.sigmoid(dot_t(rows, disp[...]))
     s0, s1 = scores[:, 0:1], scores[:, 1:2]
     mine = jnp.where(member[0] == 0, s0, s1) / (s0 + s1)
     weight[...] = jnp.broadcast_to(mine, weight.shape)
-
-
-def down_body(at, keep, near, weight, *refs):
-    downs, outs, rows = refs[:4], refs[4:8], refs[8]
+    for tile in range(4):
+        cols = slice(512 * tile, 512 * tile + 512)
+        out = dot(hidden[:, :256], downs[0][:, cols]) + dot(hidden[:, 256:], downs[1][:, cols])
+        part[:, cols] = out.astype(BF16)
+
+
+def down_body(at, part, near, weight, d0, d1, *refs):
+    outs, rows = refs[:4], refs[4]
     shift = at[0]
     for i in range(4):
-        here = slice(48 * i, 48 * i + 48)
-        rows[here, :512] = keep[here, :]
-        rows[here, 512:] = near[pl.ds(pl.multiple_of(((i + shift) % 4) * 48, 16), 48), :]
+        there = pl.ds(pl.multiple_of(((i + shift) % 4) * 48, 16), 48)
+        rows[48 * i : 48 * i + 48, :] = near[there, :]
     scale = weight[:, 0:1]
     for tile in range(4):
         cols = slice(512 * tile, 512 * tile + 512)
-        part, first = 0.0, 0
-        for d in downs:
-            part = part + dot(rows[:, first : first + d.shape[0]], d[:, cols])
-            first += d.shape[0]
-        part = (part * scale).astype(BF16)
+        out = dot(rows[:, :256], d0[:, cols]) + dot(rows[:, 256:], d1[:, cols])
+        out = ((part[:, cols] + out) * scale).astype(BF16)
         for i in range(4):
-            outs[i][:, cols] = part[48 * i : 48 * i + 48]
+            outs[i][:, cols] = out[48 * i : 48 * i + 48]
 
 
 def total_body(p0, p1, p2, p3, out):
@@ -317,34 +319,34 @@
 def experts(chunk, dispatcher, shift, ups, downs):
     own, r1, r2, r3, far, l3, l2, l1 = ring_gather(chunk)
     hidden = jax.ShapeDtypeStruct((192, 512), BF16)
-    give = call(
+    give, early = call(
         odd_body,
-        hidden,
-        (r1, r3, l3, l1, *ups),
+        (hidden, jax.ShapeDtypeStruct((144, 2048), BF16)),
+        (r1, r3, l3, l1, own, r2, l2, *ups),
         scratch=[pltpu.VMEM((192, 2048), BF16)],
         flops=4 * 192 * 2048 * 512,
         moved=6 << 20,
         limit=12,
     )
     near = neighbour(give)
-    keep, weight = call(
+    part, weight = call(
         even_body,
-        (hidden, jax.ShapeDtypeStruct((192, 128), F32)),
-        ((lax.axis_index("z") // 4)[None], own, r2, far, l2, dispatcher, *ups),
-        scratch=[pltpu.VMEM((192, 2048), BF16)],
+        (jax.ShapeDtypeStruct((192, 2048), BF16), jax.ShapeDtypeStruct((192, 128), F32)),
+        ((lax.axis_index("z") // 4)[None], early, far, dispatcher, *ups, *downs[:2]),
+        scratch=[pltpu.VMEM((192, 2048), BF16), pltpu.VMEM((192, 512), BF16)],
         specs=[SMEM] + [VMEM] * 9,
-        flops=4 * 192 * 2048 * 512,
-        moved=6 << 20,
-        limit=12,
+        flops=6 * 192 * 2048 * 512,
+        moved=8 << 20,
+        limit=16,
     )
     outs = call(
         down_body,
         tuple(jax.ShapeDtypeStruct((48, 2048), BF16) for _ in range(4)),
-        (shift, keep, near, weight, *downs),
-        scratch=[pltpu.VMEM((192, 1024), BF16)],
-        specs=[SMEM] + [VMEM] * 7,
-        flops=2 * 192 * 1024 * 2048,
-        moved=6 << 20,
+        (shift, part, near, weight, *downs[2:]),
+        scratch=[pltpu.VMEM((192, 512), BF16)],
+        specs=[SMEM] + [VMEM] * 5,
+        flops=2 * 192 * 512 * 2048,
+        moved=5 << 20,
         limit=12,
     )
     return call(

time: 160 us -> 159 us (level)
  blocking collectives: 27.4 us -> 11.3 us
  waiting for transfers between devices: 55.5 us -> 64.5 us
  starting transfers between devices: 45 us -> 52.1 us
    all_to_all x1 -> x0, blocking collectives: 16 us -> none  [shards(): lax.all_to_all(sent.reshape(groups, capacity, -1), ('y', 'x'), 0, 0, tile...]
    all_to_all x0 -> x1, waiting for transfers between devices: none -> 8.63 us  [shards(): lax.all_to_all(sent.reshape(groups, capacity, -1), ('y', 'x'), 0, 0, tile...]
    all_to_all x0 -> x1, starting transfers between devices: none -> 7.08 us  [shards(): lax.all_to_all(sent.reshape(groups, capacity, -1), ('y', 'x'), 0, 0, tile...]
    ppermute x4, waiting for transfers between devices: 11.9 us -> 15.1 us  [neighbour(): return lax.ppermute(v, 'z', [(i, i ^ 1) for i in range(8)])]
    ppermute x19, starting transfers between devices: 41.2 us -> 38 us  [shifted(): return lax.ppermute(v, axis, [(i, (i + by) % n) for i in range(n)])]
    ppermute x4, starting transfers between devices: 3.47 us -> 6.29 us  [neighbour(): return lax.ppermute(v, 'z', [(i, i ^ 1) for i in range(8)])]
    ppermute x19, waiting for transfers between devices: 42.4 us -> 39.9 us  [shifted(): return lax.ppermute(v, axis, [(i, (i + by) % n) for i in range(n)])]
    unnamed x38 -> x36, local copies, waits for them, and re-layouts: 7.55 us -> 6.53 us
  transfers between devices with their start and end apart: 30 -> 31, of which waited for: 17 -> 19; matrix products, arithmetic and copies ran while one was open for 1% -> 1% of each run, Pallas kernels for 7% -> 8%
where the time goes in v1:
time: 159 us; the launch traced here: 158 us
  waiting for transfers between devices  64.5 us (41%)
  starting transfers between devices  52.1 us (33%)
  Pallas kernels  20.1 us (13%)
  blocking collectives  11.3 us (7%)
  local copies, waits for them, and re-layouts  8.77 us (6%)
    ppermute x19, waiting for transfers between devices, shifted(): return lax.ppermute(v, axis, [(i, (i + by) % n) for i in range(n)])  39.9 us
    ppermute x19, starting transfers between devices, shifted(): return lax.ppermute(v, axis, [(i, (i + by) % n) for i in range(n)])  38 us
    pallas_call x10, Pallas kernels, call(): pl.pallas_call(body, out_shape=outs, in_specs=specs or [VMEM] * len(args)...  20.1 us
    ppermute x4, waiting for transfers between devices, neighbour(): return lax.ppermute(v, 'z', [(i, i ^ 1) for i in range(8)])  15.1 us
    all_to_all x1, blocking collectives, shards(): lax.all_to_all(summed.reshape(groups, capacity, -1), ('y', 'x'), 0, 0, ti...  11.3 us
    all_to_all x1, waiting for transfers between devices, shards(): lax.all_to_all(sent.reshape(groups, capacity, -1), ('y', 'x'), 0, 0, tile...  8.63 us
    all_to_all x1, starting transfers between devices, shards(): lax.all_to_all(sent.reshape(groups, capacity, -1), ('y', 'x'), 0, 0, tile...  7.08 us
    unnamed x36, local copies, waits for them, and re-layouts  6.53 us
  transfers between devices with their start and end apart: 31, of which 19 were waited for; matrix products, arithmetic and copies ran while one was open for 1% of the time, Pallas kernels for 8%

profile of v1, /device:TPU:32, one launch (start us, length us, event | category | flops | bytes accessed | tf_op | source)
XLA Modules:
  0.0 158.3 jit_solution(608658153336907046)
XLA Ops:
  0.0 5.5 %shard_map.199 = (bf16[80,384]{1,0:T(8,128)(2,1)}, bf16[1024,384]{1,0:T(8,128)(2,1)}, bf16[128,2048]{1,0:T(8,128)(2,1)}) custom-call(bf16[512,128]{1,0:T(8,128)(2,1)} %refs_0_.1, bf16[512,128]{1,0:T(8,128)(2,1)} %refs_1_.1, bf16[512,256]{1,0:T(8,128)(2,1)} %refs_2_.1, bf16[512,256]{1,0:T(8,128)(2,1)} %refs_3_.1, bf16[512,128]{1,0:T(8,128)(2,1)} %values.1, ...), custom_call_target="tpu_custom_call" | custom-call | flops 603979776 | bytes 3145728 | tf_op jit(solution)/shard_map/pallas_call | solution.py:45
  5.5 1.9 %collective-permute-start.9 = (bf16[128,2048]{1,0:T(8,128)(2,1)}, bf16[128,2048]{1,0:T(8,128)(2,1)}, u32[]{:S(2)}, u32[]{:S(2)}) collective-permute-start(bf16[128,2048]{1,0:T(8,128)(2,1)} %get-tuple-element.32.w0), channel_id=1, source_target_pairs={{0,2},{2,0},{4,6},{6,4},{8,10},{10,8},{12,14},{14,12},{1,3},{3,1},... | collective-permute-start | bytes 1572872 | tf_op jit(solution)/shard_map/ppermute | solution.py:57
  7.4 1.7 %collective-permute-start.25 = (bf16[256,2048]{1,0:T(8,128)(2,1)}, bf16[256,2048]{1,0:T(8,128)(2,1)}, u32[]{:S(2)}, u32[]{:S(2)}) collective-permute-start(bf16[256,2048]{1,0:T(8,128)(2,1)} %bitcast.19.refs_7_), channel_id=1, source_target_pairs={{0,2},{2,0},{4,6},{6,4},{8,10},{10,8},{12,14},{14,12},{1,3},{3,1},... | collective-permute-start | bytes 3145736 | tf_op jit(solution)/shard_map/ppermute | solution.py:57
  9.1 2.7 %collective-permute-start.1 = (bf16[80,384]{1,0:T(8,128)(2,1)}, bf16[80,384]{1,0:T(8,128)(2,1)S(1)}, u32[]{:S(2)}, u32[]{:S(2)}) collective-permute-start(bf16[80,384]{1,0:T(8,128)(2,1)} %get-tuple-element.27.own), channel_id=1, source_target_pairs={{0,32},{16,48},{32,0},{48,16},{1,33},{17,49},{33,1},{49,17},{2,34}... | collective-permute-start | bytes 184328 | tf_op jit(solution)/shard_map/ppermute | solution.py:19
  11.8 1.4 collective-permute-start.2
  13.3 0.4 collective-permute-done.got1
  13.7 7.0 %collective-permute-done.9.w2 = bf16[128,2048]{1,0:T(8,128)(2,1)} collective-permute-done((bf16[128,2048]{1,0:T(8,128)(2,1)}, bf16[128,2048]{1,0:T(8,128)(2,1)}, u32[]{:S(2)}, u32[]{:S(2)}) %collective-permute-start.9) | collective-permute-done | bytes 524320 | tf_op jit(solution)/shard_map/ppermute | solution.py:57
  20.8 0.8 copy-done.11
  21.6 0.7 shard_map.200
  22.3 1.6 %collective-permute-start.3 = (bf16[80,384]{1,0:T(8,128)(2,1)S(1)}, bf16[80,384]{1,0:T(8,128)(2,1)S(1)}, u32[]{:S(2)}, u32[]{:S(2)}) collective-permute-start(bf16[80,384]{1,0:T(8,128)(2,1)S(1)} %get-tuple-element.29), channel_id=1, source_target_pairs={{0,64},{64,128},{128,192},{192,0},{1,65},{65,129},{129,193},{193,1... | collective-permute-start | bytes 184328 | tf_op jit(solution)/shard_map/ppermute | solution.py:19
  24.0 2.9 %collective-permute-start.4 = (bf16[80,384]{1,0:T(8,128)(2,1)S(1)}, bf16[80,384]{1,0:T(8,128)(2,1)S(1)}, u32[]{:S(2)}, u32[]{:S(2)}) collective-permute-start(bf16[80,384]{1,0:T(8,128)(2,1)S(1)} %get-tuple-element.29), channel_id=1, source_target_pairs={{0,128},{64,192},{128,0},{192,64},{1,129},{65,193},{129,1},{193,65... | collective-permute-start | bytes 184328 | tf_op jit(solution)/shard_map/ppermute | solution.py:19
  26.9 1.2 collective-permute-done.3.got1
  28.1 2.2 %collective-permute-start.5 = (bf16[80,384]{1,0:T(8,128)(2,1)S(1)}, bf16[80,384]{1,0:T(8,128)(2,1)S(1)}, u32[]{:S(2)}, u32[]{:S(2)}) collective-permute-start(bf16[80,384]{1,0:T(8,128)(2,1)S(1)} %get-tuple-element.29), channel_id=1, source_target_pairs={{0,192},{64,0},{128,64},{192,128},{1,193},{65,1},{129,65},{193,129... | collective-permute-start | bytes 184328 | tf_op jit(solution)/shard_map/ppermute | solution.py:19
  30.3 0.3 collective-permute-done.4.got2
  30.6 1.1 copy-done.2
  31.8 0.9 shard_map.201.intra
  32.7 1.7 %shard_map.202 = (bf16[256,128]{1,0:T(8,128)(2,1)S(1)}, bf16[256,128]{1,0:T(8,128)(2,1)S(1)}) custom-call(s32[4]{0:T(128)S(1)} %pad_add_fusion.at, bf16[1024,384]{1,0:T(8,128)(2,1)S(1)} %copy-done.2, f32[72,384]{1,0:T(8,128)S(1)} %get-tuple-element.28.before, bf16[80,384]{1,0:T(8,128)(2,1)S(1)} %collective-permute-done.3.got1, ...), custom_call_target="tpu_custom_call" | custom-call | flops 25165824 | bytes 1048576 | tf_op jit(solution)/shard_map/pallas_call | solution.py:45
  34.4 0.6 collective-permute-start.6
  35.0 0.9 collective-permute-done.6.got
  35.9 2.7 %collective-permute-start.7 = (bf16[128,256]{1,0:T(8,128)(2,1)S(1)}, bf16[128,256]{1,0:T(8,128)(2,1)S(1)}, u32[]{:S(2)}, u32[]{:S(2)}) collective-permute-start(bf16[128,256]{1,0:T(8,128)(2,1)S(1)} %pad_maximum_fusion), channel_id=1, source_target_pairs={{0,2},{2,0},{4,6},{6,4},{8,10},{10,8},{12,14},{14,12},{1,3},{3,1},... | collective-permute-start | bytes 196616 | tf_op jit(solution)/shard_map/ppermute | solution.py:57
  38.6 4.7 %collective-permute-done.7.near = bf16[128,256]{1,0:T(8,128)(2,1)S(1)} collective-permute-done((bf16[128,256]{1,0:T(8,128)(2,1)S(1)}, bf16[128,256]{1,0:T(8,128)(2,1)S(1)}, u32[]{:S(2)}, u32[]{:S(2)}) %collective-permute-start.7) | collective-permute-done | bytes 65568 | tf_op jit(solution)/shard_map/ppermute | solution.py:57
  43.4 1.0 copy-done.5
  44.4 2.1 %shard_map.203 = (bf16[32,2048]{1,0:T(8,128)(2,1)S(1)}, bf16[32,2048]{1,0:T(8,128)(2,1)S(1)}, bf16[32,2048]{1,0:T(8,128)(2,1)S(1)}, bf16[32,2048]{1,0:T(8,128)(2,1)S(1)}) custom-call(s32[1]{0:T(128)} %bitcast.at, bf16[256,128]{1,0:T(8,128)(2,1)S(1)} %get-tuple-element.30.keep, bf16[256,128]{1,0:T(8,128)(2,1)S(1)} %collective-permute-done.6.got, ...), custom_call_target="tpu_custom_call" | custom-call | flops 268435456 | bytes 4194304 | tf_op jit(solution)/shard_map/pallas_call | solution.py:45
  46.5 3.4 %collective-permute-start.11 = (bf16[32,2048]{1,0:T(8,128)(2,1)S(1)}, bf16[32,2048]{1,0:T(8,128)(2,1)S(1)}, u32[]{:S(2)}, u32[]{:S(2)}) collective-permute-start(bf16[32,2048]{1,0:T(8,128)(2,1)S(1)} %get-tuple-element.34), channel_id=1, source_target_pairs={{0,4},{2,6},{4,8},{6,10},{8,12},{10,14},{12,0},{14,2},{1,5},{3,7},... | collective-permute-start | bytes 393224 | tf_op jit(solution)/shard_map/ppermute | solution.py:19
  49.9 2.2 %collective-permute-start.12 = (bf16[32,2048]{1,0:T(8,128)(2,1)S(1)}, bf16[32,2048]{1,0:T(8,128)(2,1)S(1)}, u32[]{:S(2)}, u32[]{:S(2)}) collective-permute-start(bf16[32,2048]{1,0:T(8,128)(2,1)S(1)} %get-tuple-element.35), channel_id=1, source_target_pairs={{0,12},{2,14},{4,0},{6,2},{8,4},{10,6},{12,8},{14,10},{1,13},{3,15... | collective-permute-start | bytes 393224 | tf_op jit(solution)/shard_map/ppermute | solution.py:19
  52.1 6.9 %collective-permute-done.11.p1 = bf16[32,2048]{1,0:T(8,128)(2,1)S(1)} collective-permute-done((bf16[32,2048]{1,0:T(8,128)(2,1)S(1)}, bf16[32,2048]{1,0:T(8,128)(2,1)S(1)}, u32[]{:S(2)}, u32[]{:S(2)}) %collective-permute-start.11) | collective-permute-done | bytes 131104 | tf_op jit(solution)/shard_map/ppermute | solution.py:19
  59.0 3.1 %collective-permute-start.13 = (bf16[32,2048]{1,0:T(8,128)(2,1)S(1)}, bf16[32,2048]{1,0:T(8,128)(2,1)S(1)}, u32[]{:S(2)}, u32[]{:S(2)}) collective-permute-start(bf16[32,2048]{1,0:T(8,128)(2,1)S(1)} %get-tuple-element.36), channel_id=1, source_target_pairs={{0,8},{2,10},{4,12},{6,14},{8,0},{10,2},{12,4},{14,6},{1,9},{3,11}... | collective-permute-start | bytes 393224 | tf_op jit(solution)/shard_map/ppermute | solution.py:19
  62.1 7.8 %collective-permute-done.13.p3 = bf16[32,2048]{1,0:T(8,128)(2,1)S(1)} collective-permute-done((bf16[32,2048]{1,0:T(8,128)(2,1)S(1)}, bf16[32,2048]{1,0:T(8,128)(2,1)S(1)}, u32[]{:S(2)}, u32[]{:S(2)}) %collective-permute-start.13) | collective-permute-done | bytes 131104 | tf_op jit(solution)/shard_map/ppermute | solution.py:19
  69.9 0.5 shard_map.204
  70.4 0.6 copy-done.8
  71.0 0.8 reshape.32
  71.8 7.1 %all-to-all-start = ((bf16[16,3,2048]{2,1,0:T(4,128)(2,1)}), bf16[16,3,2048]{2,1,0:T(4,128)(2,1)}, u32[]{:S(2)}, u32[]{:S(2)}) async-start(bf16[16,3,2048]{2,1,0:T(4,128)(2,1)} %reshape.32), calls=%async_computation | async-start | bytes 524288 | tf_op jit(solution)/shard_map/all_to_all | solution.py:389
  79.1 8.6 %all-to-all-done = bf16[16,3,2048]{2,1,0:T(4,128)(2,1)} async-done(((bf16[16,3,2048]{2,1,0:T(4,128)(2,1)}), bf16[16,3,2048]{2,1,0:T(4,128)(2,1)}, u32[]{:S(2)}, u32[]{:S(2)}) %all-to-all-start) | async-done | bytes 196640 | tf_op jit(solution)/shard_map/all_to_all | solution.py:389
  87.7 1.1 reshape.33.refs_4_
  88.8 4.0 %collective-permute-start.17 = (bf16[48,2048]{1,0:T(8,128)(2,1)S(1)}, bf16[48,2048]{1,0:T(8,128)(2,1)S(1)}, u32[]{:S(2)}, u32[]{:S(2)}) collective-permute-start(bf16[48,2048]{1,0:T(8,128)(2,1)S(1)} %reshape.33.refs_4_), channel_id=1, source_target_pairs={{0,2},{2,4},{4,6},{6,8},{8,10},{10,12},{12,14},{14,0},{1,3},{3,5},... | collective-permute-start | bytes 589832 | tf_op jit(solution)/shard_map/ppermute | solution.py:19
  92.9 3.5 %collective-permute-done.17.refs_3_ = bf16[48,2048]{1,0:T(8,128)(2,1)S(1)} collective-permute-done((bf16[48,2048]{1,0:T(8,128)(2,1)S(1)}, bf16[48,2048]{1,0:T(8,128)(2,1)S(1)}, u32[]{:S(2)}, u32[]{:S(2)}) %collective-permute-start.17) | collective-permute-done | bytes 196640 | tf_op jit(solution)/shard_map/ppermute | solution.py:19
  96.3 2.5 %collective-permute-start.18 = (bf16[48,2048]{1,0:T(8,128)(2,1)S(1)}, bf16[48,2048]{1,0:T(8,128)(2,1)S(1)}, u32[]{:S(2)}, u32[]{:S(2)}) collective-permute-start(bf16[48,2048]{1,0:T(8,128)(2,1)S(1)} %collective-permute-done.17.refs_3_), channel_id=1, source_target_pairs={{0,2},{2,4},{4,6},{6,8},{8,10},{10,12},{12,14},{14,0},{1,3},{3,5},... | collective-permute-start | bytes 589832 | tf_op jit(solution)/shard_map/ppermute | solution.py:19
  98.8 0.3 collective-permute-done.14.refs_0_
  99.1 4.3 %collective-permute-done.18.refs_6_ = bf16[48,2048]{1,0:T(8,128)(2,1)S(1)} collective-permute-done((bf16[48,2048]{1,0:T(8,128)(2,1)S(1)}, bf16[48,2048]{1,0:T(8,128)(2,1)S(1)}, u32[]{:S(2)}, u32[]{:S(2)}) %collective-permute-start.18) | collective-permute-done | bytes 196640 | tf_op jit(solution)/shard_map/ppermute | solution.py:19
  103.4 2.5 %collective-permute-start.19 = (bf16[48,2048]{1,0:T(8,128)(2,1)S(1)}, bf16[48,2048]{1,0:T(8,128)(2,1)S(1)}, u32[]{:S(2)}, u32[]{:S(2)}) collective-permute-start(bf16[48,2048]{1,0:T(8,128)(2,1)S(1)} %collective-permute-done.18.refs_6_), channel_id=1, source_target_pairs={{0,2},{2,4},{4,6},{6,8},{8,10},{10,12},{12,14},{14,0},{1,3},{3,5},... | collective-permute-start | bytes 589832 | tf_op jit(solution)/shard_map/ppermute | solution.py:19
  105.9 0.3 collective-permute-done.15.refs_5_
  106.2 4.8 %collective-permute-done.19.refs_2_ = bf16[48,2048]{1,0:T(8,128)(2,1)S(1)} collective-permute-done((bf16[48,2048]{1,0:T(8,128)(2,1)S(1)}, bf16[48,2048]{1,0:T(8,128)(2,1)S(1)}, u32[]{:S(2)}, u32[]{:S(2)}) %collective-permute-start.19) | collective-permute-done | bytes 196640 | tf_op jit(solution)/shard_map/ppermute | solution.py:19
  111.0 2.5 %collective-permute-start.22 = (bf16[48,2048]{1,0:T(8,128)(2,1)S(1)}, bf16[48,2048]{1,0:T(8,128)(2,1)}, u32[]{:S(2)}, u32[]{:S(2)}) collective-permute-start(bf16[48,2048]{1,0:T(8,128)(2,1)S(1)} %collective-permute-done.19.refs_2_), channel_id=1, source_target_pairs={{0,2},{2,4},{4,6},{6,8},{8,10},{10,12},{12,14},{14,0},{1,3},{3,5},... | collective-permute-start | bytes 589832 | tf_op jit(solution)/shard_map/ppermute | solution.py:19
  113.5 2.9 %shard_map.205 = (bf16[192,512]{1,0:T(8,128)(2,1)}, bf16[144,2048]{1,0:T(8,128)(2,1)S(1)}) custom-call(bf16[48,2048]{1,0:T(8,128)(2,1)S(1)} %collective-permute-done.14.refs_0_, bf16[48,2048]{1,0:T(8,128)(2,1)S(1)} %collective-permute-done.16.refs_1_, bf16[48,2048]{1,0:T(8,128)(2,1)S(1)} %collective-permute-done.19.refs_2_, ...), custom_call_target="tpu_custom_call" | custom-call | flops 805306368 | bytes 6291456 | tf_op jit(solution)/shard_map/pallas_call | solution.py:45
  116.5 0.8 copy-done.3
  117.3 0.3 collective-permute-done.22.refs_1_
  117.6 0.4 copy-done.14
  118.0 1.1 copy-done.4
  119.1 3.6 %shard_map.206 = (bf16[192,2048]{1,0:T(8,128)(2,1)S(1)}, f32[192,128]{1,0:T(8,128)S(1)}) custom-call(s32[1]{0:T(128)} %bitcast.15.member, bf16[144,2048]{1,0:T(8,128)(2,1)S(1)} %copy-done.4, bf16[48,2048]{1,0:T(8,128)(2,1)} %collective-permute-done.22.refs_1_, bf16[2,2048]{1,0:T(2,128)(2,1)S(1)} %bitcast.35, bf16[2048,256]{1,0:T(8,128)(2,1)S(1)} %bitcast.27, ...), custom_call_target="tpu_custom_call" | custom-call | flops 1207959552 | bytes 8388608 | tf_op jit(solution)/shard_map/pallas_call | solution.py:45
  122.7 3.4 %collective-permute-done.24.near = bf16[192,512]{1,0:T(8,128)(2,1)S(1)} collective-permute-done((bf16[192,512]{1,0:T(8,128)(2,1)}, bf16[192,512]{1,0:T(8,128)(2,1)S(1)}, u32[]{:S(2)}, u32[]{:S(2)}) %collective-permute-start.24) | collective-permute-done | bytes 196640 | tf_op jit(solution)/shard_map/ppermute | solution.py:57
  126.1 2.1 %shard_map.207 = (bf16[48,2048]{1,0:T(8,128)(2,1)S(1)}, bf16[48,2048]{1,0:T(8,128)(2,1)S(1)}, bf16[48,2048]{1,0:T(8,128)(2,1)S(1)}, bf16[48,2048]{1,0:T(8,128)(2,1)S(1)}) custom-call(s32[1]{0:T(128)} %bitcast.at, bf16[192,2048]{1,0:T(8,128)(2,1)S(1)} %get-tuple-element.40.part, bf16[192,512]{1,0:T(8,128)(2,1)S(1)} %collective-permute-done.24.near, ...), custom_call_target="tpu_custom_call" | custom-call | flops 402653184 | bytes 5242880 | tf_op jit(solution)/shard_map/pallas_call | solution.py:45
  128.2 3.3 %collective-permute-start.27 = (bf16[48,2048]{1,0:T(8,128)(2,1)S(1)}, bf16[48,2048]{1,0:T(8,128)(2,1)S(1)}, u32[]{:S(2)}, u32[]{:S(2)}) collective-permute-start(bf16[48,2048]{1,0:T(8,128)(2,1)S(1)} %get-tuple-element.44), channel_id=1, source_target_pairs={{0,4},{2,6},{4,8},{6,10},{8,12},{10,14},{12,0},{14,2},{1,5},{3,7},... | collective-permute-start | bytes 589832 | tf_op jit(solution)/shard_map/ppermute | solution.py:19
  131.5 0.9 collective-permute-start.28
  132.4 2.7 %collective-permute-start.29 = (bf16[48,2048]{1,0:T(8,128)(2,1)S(1)}, bf16[48,2048]{1,0:T(8,128)(2,1)S(1)}, u32[]{:S(2)}, u32[]{:S(2)}) collective-permute-start(bf16[48,2048]{1,0:T(8,128)(2,1)S(1)} %get-tuple-element.46), channel_id=1, source_target_pairs={{0,8},{2,10},{4,12},{6,14},{8,0},{10,2},{12,4},{14,6},{1,9},{3,11}... | collective-permute-start | bytes 589832 | tf_op jit(solution)/shard_map/ppermute | solution.py:19
  135.1 2.9 %collective-permute-done.27.p1 = bf16[48,2048]{1,0:T(8,128)(2,1)S(1)} collective-permute-done((bf16[48,2048]{1,0:T(8,128)(2,1)S(1)}, bf16[48,2048]{1,0:T(8,128)(2,1)S(1)}, u32[]{:S(2)}, u32[]{:S(2)}) %collective-permute-start.27) | collective-permute-done | bytes 196640 | tf_op jit(solution)/shard_map/ppermute | solution.py:19
  138.0 1.1 collective-permute-done.28.p2
  139.1 5.8 %collective-permute-done.29.p3 = bf16[48,2048]{1,0:T(8,128)(2,1)S(1)} collective-permute-done((bf16[48,2048]{1,0:T(8,128)(2,1)S(1)}, bf16[48,2048]{1,0:T(8,128)(2,1)S(1)}, u32[]{:S(2)}, u32[]{:S(2)}) %collective-permute-start.29) | collective-permute-done | bytes 196640 | tf_op jit(solution)/shard_map/ppermute | solution.py:19
  144.9 0.1 shard_map.208
  145.0 0.1 reshape.34
  145.1 11.3 %all_to_all.10 = bf16[16,3,2048]{2,1,0:T(4,128)(2,1)S(1)} all-to-all(bf16[16,3,2048]{2,1,0:T(4,128)(2,1)S(1)} %reshape.34), channel_id=1, replica_groups=mesh['y'=4,'x'=4,'z'=8,'core'=2] {'y','x'}, dimensions={0} | all-to-all | bytes 393216 | tf_op jit(solution)/shard_map/all_to_all | solution.py:394
  156.4 0.2 reshape.35
  156.6 0.3 multiply_reduce_fusion
  157.0 0.5 copy-done.9
  157.5 0.8 add_convert_fusion
  (59 shorter events, 0.4 us)
Async XLA Ops:
  0.0 30.6 %copy-start = (bf16[1,2048,256]{2,1,0:T(8,128)(2,1)S(1)}, bf16[1,2048,256]{2,1,0:T(8,128)(2,1)}, u32[]{:S(2)}) copy-start(bf16[1,2048,256]{2,1,0:T(8,128)(2,1)} %param.38) | copy-start | bytes 3145732
  5.5 15.2 %collective-permute-start.9 = (bf16[128,2048]{1,0:T(8,128)(2,1)}, bf16[128,2048]{1,0:T(8,128)(2,1)}, u32[]{:S(2)}, u32[]{:S(2)}) collective-permute-start(bf16[128,2048]{1,0:T(8,128)(2,1)} %get-tuple-element.32.w0), channel_id=1, source_target_pairs={{0,2},{2,0},{4,6},{6,4},{8,10},{10,8},{12,14},{14,12},{1,3},{3,1},... | collective-permute-start | bytes 1572872 | tf_op jit(solution)/shard_map/ppermute | solution.py:57
  7.4 6.3 %collective-permute-start = (bf16[80,384]{1,0:T(8,128)(2,1)}, bf16[80,384]{1,0:T(8,128)(2,1)S(1)}, u32[]{:S(2)}, u32[]{:S(2)}) collective-permute-start(bf16[80,384]{1,0:T(8,128)(2,1)} %get-tuple-element.27.own), channel_id=1, source_target_pairs={{0,16},{16,32},{32,48},{48,0},{1,17},{17,33},{33,49},{49,1},{2,18}... | collective-permute-start | bytes 184328 | tf_op jit(solution)/shard_map/ppermute | solution.py:19
  7.4 71.5 %collective-permute-start.25 = (bf16[256,2048]{1,0:T(8,128)(2,1)}, bf16[256,2048]{1,0:T(8,128)(2,1)}, u32[]{:S(2)}, u32[]{:S(2)}) collective-permute-start(bf16[256,2048]{1,0:T(8,128)(2,1)} %bitcast.19.refs_7_), channel_id=1, source_target_pairs={{0,2},{2,0},{4,6},{6,4},{8,10},{10,8},{12,14},{14,12},{1,3},{3,1},... | collective-permute-start | bytes 3145736 | tf_op jit(solution)/shard_map/ppermute | solution.py:57
  9.1 11.7 %collective-permute-start.1 = (bf16[80,384]{1,0:T(8,128)(2,1)}, bf16[80,384]{1,0:T(8,128)(2,1)S(1)}, u32[]{:S(2)}, u32[]{:S(2)}) collective-permute-start(bf16[80,384]{1,0:T(8,128)(2,1)} %get-tuple-element.27.own), channel_id=1, source_target_pairs={{0,32},{16,48},{32,0},{48,16},{1,33},{17,49},{33,1},{49,17},{2,34}... | collective-permute-start | bytes 184328 | tf_op jit(solution)/shard_map/ppermute | solution.py:19
  11.8 9.0 %collective-permute-start.2 = (bf16[80,384]{1,0:T(8,128)(2,1)}, bf16[80,384]{1,0:T(8,128)(2,1)S(1)}, u32[]{:S(2)}, u32[]{:S(2)}) collective-permute-start(bf16[80,384]{1,0:T(8,128)(2,1)} %get-tuple-element.27.own), channel_id=1, source_target_pairs={{0,48},{16,0},{32,16},{48,32},{1,49},{17,1},{33,17},{49,33},{2,50}... | collective-permute-start | bytes 184328 | tf_op jit(solution)/shard_map/ppermute | solution.py:19
  13.3 17.3 %copy-start.6 = (bf16[512,128]{1,0:T(8,128)(2,1)S(1)}, bf16[512,128]{1,0:T(8,128)(2,1)}, u32[]{:S(2)}) copy-start(bf16[512,128]{1,0:T(8,128)(2,1)} %values.1) | copy-start | bytes 393220
  13.7 29.6 %collective-permute-start.8 = (bf16[128,2048]{1,0:T(8,128)(2,1)}, bf16[128,2048]{1,0:T(8,128)(2,1)}, u32[]{:S(2)}, u32[]{:S(2)}) collective-permute-start(bf16[128,2048]{1,0:T(8,128)(2,1)} %get-tuple-element.32.w0), channel_id=1, source_target_pairs={{0,1},{1,0},{2,3},{3,2},{4,5},{5,4},{6,7},{7,6},{8,9},{9,8},{10,11... | collective-permute-start | bytes 1572872 | tf_op jit(solution)/shard_map/ppermute | solution.py:23
  20.7 22.6 %collective-permute-start.10 = (bf16[128,2048]{1,0:T(8,128)(2,1)}, bf16[128,2048]{1,0:T(8,128)(2,1)}, u32[]{:S(2)}, u32[]{:S(2)}) collective-permute-start(bf16[128,2048]{1,0:T(8,128)(2,1)} %collective-permute-done.9.w2), channel_id=1, source_target_pairs={{0,1},{1,0},{2,3},{3,2},{4,5},{5,4},{6,7},{7,6},{8,9},{9,8},{10,11... | collective-permute-start | bytes 1572872 | tf_op jit(solution)/shard_map/ppermute | solution.py:23
  20.8 0.8 copy-start.11
  22.3 5.8 %collective-permute-start.3 = (bf16[80,384]{1,0:T(8,128)(2,1)S(1)}, bf16[80,384]{1,0:T(8,128)(2,1)S(1)}, u32[]{:S(2)}, u32[]{:S(2)}) collective-permute-start(bf16[80,384]{1,0:T(8,128)(2,1)S(1)} %get-tuple-element.29), channel_id=1, source_target_pairs={{0,64},{64,128},{128,192},{192,0},{1,65},{65,129},{129,193},{193,1... | collective-permute-start | bytes 184328 | tf_op jit(solution)/shard_map/ppermute | solution.py:19
  24.0 6.6 %collective-permute-start.4 = (bf16[80,384]{1,0:T(8,128)(2,1)S(1)}, bf16[80,384]{1,0:T(8,128)(2,1)S(1)}, u32[]{:S(2)}, u32[]{:S(2)}) collective-permute-start(bf16[80,384]{1,0:T(8,128)(2,1)S(1)} %get-tuple-element.29), channel_id=1, source_target_pairs={{0,128},{64,192},{128,0},{192,64},{1,129},{65,193},{129,1},{193,65... | collective-permute-start | bytes 184328 | tf_op jit(solution)/shard_map/ppermute | solution.py:19
  28.1 4.5 %collective-permute-start.5 = (bf16[80,384]{1,0:T(8,128)(2,1)S(1)}, bf16[80,384]{1,0:T(8,128)(2,1)S(1)}, u32[]{:S(2)}, u32[]{:S(2)}) collective-permute-start(bf16[80,384]{1,0:T(8,128)(2,1)S(1)} %get-tuple-element.29), channel_id=1, source_target_pairs={{0,192},{64,0},{128,64},{192,128},{1,193},{65,1},{129,65},{193,129... | collective-permute-start | bytes 184328 | tf_op jit(solution)/shard_map/ppermute | solution.py:19
  30.6 62.2 %collective-permute-start.20 = (bf16[2048,256]{1,0:T(8,128)(2,1)S(1)}, bf16[2048,256]{1,0:T(8,128)(2,1)S(1)}, u32[]{:S(2)}, u32[]{:S(2)}) collective-permute-start(bf16[2048,256]{1,0:T(8,128)(2,1)S(1)} %bitcast.25), channel_id=1, source_target_pairs={{0,1},{1,0},{2,3},{3,2},{4,5},{5,4},{6,7},{7,6},{8,9},{9,8},{10,11... | collective-permute-start | bytes 3145736 | tf_op jit(solution)/shard_map/ppermute | solution.py:23
  30.6 1.1 copy-start.2
  31.7 0.9 copy-start.7
  31.7 0.9 copy-start.15
  32.6 10.7 %copy-start.1 = (bf16[1,2048,256]{2,1,0:T(8,128)(2,1)S(1)}, bf16[1,2048,256]{2,1,0:T(8,128)(2,1)}, u32[]{:S(2)}) copy-start(bf16[1,2048,256]{2,1,0:T(8,128)(2,1)} %param.39) | copy-start | bytes 3145732
  34.4 1.5 collective-permute-start.6
  35.9 2.7 %copy-start.17 = (s32[32]{0:T(128)S(1)}, s32[32]{0:T(128)}, u32[]{:S(2)}) copy-start(s32[32]{0:T(128)} %param.41) | copy-start | bytes 388
  35.9 7.5 %collective-permute-start.7 = (bf16[128,256]{1,0:T(8,128)(2,1)S(1)}, bf16[128,256]{1,0:T(8,128)(2,1)S(1)}, u32[]{:S(2)}, u32[]{:S(2)}) collective-permute-start(bf16[128,256]{1,0:T(8,128)(2,1)S(1)} %pad_maximum_fusion), channel_id=1, source_target_pairs={{0,2},{2,0},{4,6},{6,4},{8,10},{10,8},{12,14},{14,12},{1,3},{3,1},... | collective-permute-start | bytes 196616 | tf_op jit(solution)/shard_map/ppermute | solution.py:57
  43.3 70.2 %collective-permute-start.21 = (bf16[2048,256]{1,0:T(8,128)(2,1)S(1)}, bf16[2048,256]{1,0:T(8,128)(2,1)}, u32[]{:S(2)}, u32[]{:S(2)}) collective-permute-start(bf16[2048,256]{1,0:T(8,128)(2,1)S(1)} %bitcast.28), channel_id=1, source_target_pairs={{0,1},{1,0},{2,3},{3,2},{4,5},{5,4},{6,7},{7,6},{8,9},{9,8},{10,11... | collective-permute-start | bytes 3145736 | tf_op jit(solution)/shard_map/ppermute | solution.py:23
  43.4 1.0 copy-start.5
  44.4 25.5 %copy-start.10 = (bf16[32,2048]{1,0:T(8,128)(2,1)S(1)}, bf16[32,2048]{1,0:T(8,128)(2,1)}, u32[]{:S(2)}) copy-start(bf16[32,2048]{1,0:T(8,128)(2,1)} %skip.1) | copy-start | bytes 393220
  46.5 12.4 %collective-permute-start.11 = (bf16[32,2048]{1,0:T(8,128)(2,1)S(1)}, bf16[32,2048]{1,0:T(8,128)(2,1)S(1)}, u32[]{:S(2)}, u32[]{:S(2)}) collective-permute-start(bf16[32,2048]{1,0:T(8,128)(2,1)S(1)} %get-tuple-element.34), channel_id=1, source_target_pairs={{0,4},{2,6},{4,8},{6,10},{8,12},{10,14},{12,0},{14,2},{1,5},{3,7},... | collective-permute-start | bytes 393224 | tf_op jit(solution)/shard_map/ppermute | solution.py:19
  49.9 9.1 %collective-permute-start.12 = (bf16[32,2048]{1,0:T(8,128)(2,1)S(1)}, bf16[32,2048]{1,0:T(8,128)(2,1)S(1)}, u32[]{:S(2)}, u32[]{:S(2)}) collective-permute-start(bf16[32,2048]{1,0:T(8,128)(2,1)S(1)} %get-tuple-element.35), channel_id=1, source_target_pairs={{0,12},{2,14},{4,0},{6,2},{8,4},{10,6},{12,8},{14,10},{1,13},{3,15... | collective-permute-start | bytes 393224 | tf_op jit(solution)/shard_map/ppermute | solution.py:19
  59.0 58.3 %collective-permute-start.23 = (bf16[256,2048]{1,0:T(8,128)(2,1)}, bf16[256,2048]{1,0:T(8,128)(2,1)}, u32[]{:S(2)}, u32[]{:S(2)}) collective-permute-start(bf16[256,2048]{1,0:T(8,128)(2,1)} %bitcast.19.refs_7_), channel_id=1, source_target_pairs={{0,1},{1,0},{2,3},{3,2},{4,5},{5,4},{6,7},{7,6},{8,9},{9,8},{10,11... | collective-permute-start | bytes 3145736 | tf_op jit(solution)/shard_map/ppermute | solution.py:23
  59.0 10.9 %copy-start.12 = (f32[2048]{0:T(1024)S(1)}, f32[2048]{0:T(1024)}, u32[]{:S(2)}) copy-start(f32[2048]{0:T(1024)} %param.34) | copy-start | bytes 24580
  59.0 10.9 %copy-start.13 = (f32[2048]{0:T(1024)S(1)}, f32[2048]{0:T(1024)}, u32[]{:S(2)}) copy-start(f32[2048]{0:T(1024)} %param.35) | copy-start | bytes 24580
  59.0 10.9 %collective-permute-start.13 = (bf16[32,2048]{1,0:T(8,128)(2,1)S(1)}, bf16[32,2048]{1,0:T(8,128)(2,1)S(1)}, u32[]{:S(2)}, u32[]{:S(2)}) collective-permute-start(bf16[32,2048]{1,0:T(8,128)(2,1)S(1)} %get-tuple-element.36), channel_id=1, source_target_pairs={{0,8},{2,10},{4,12},{6,14},{8,0},{10,2},{12,4},{14,6},{1,9},{3,11}... | collective-permute-start | bytes 393224 | tf_op jit(solution)/shard_map/ppermute | solution.py:19
  70.4 0.7 copy-start.8
  71.8 15.8 %all-to-all-start = ((bf16[16,3,2048]{2,1,0:T(4,128)(2,1)}), bf16[16,3,2048]{2,1,0:T(4,128)(2,1)}, u32[]{:S(2)}, u32[]{:S(2)}) async-start(bf16[16,3,2048]{2,1,0:T(4,128)(2,1)} %reshape.32), calls=%async_computation | async-start | bytes 524288 | tf_op jit(solution)/shard_map/all_to_all | solution.py:389
  78.9 43.7 %collective-permute-start.26 = (bf16[256,2048]{1,0:T(8,128)(2,1)}, bf16[256,2048]{1,0:T(8,128)(2,1)}, u32[]{:S(2)}, u32[]{:S(2)}) collective-permute-start(bf16[256,2048]{1,0:T(8,128)(2,1)} %collective-permute-done.25.d0), channel_id=1, source_target_pairs={{0,1},{1,0},{2,3},{3,2},{4,5},{5,4},{6,7},{7,6},{8,9},{9,8},{10,11... | collective-permute-start | bytes 3145736 | tf_op jit(solution)/shard_map/ppermute | solution.py:23
  88.8 7.5 %collective-permute-start.17 = (bf16[48,2048]{1,0:T(8,128)(2,1)S(1)}, bf16[48,2048]{1,0:T(8,128)(2,1)S(1)}, u32[]{:S(2)}, u32[]{:S(2)}) collective-permute-start(bf16[48,2048]{1,0:T(8,128)(2,1)S(1)} %reshape.33.refs_4_), channel_id=1, source_target_pairs={{0,2},{2,4},{4,6},{6,8},{8,10},{10,12},{12,14},{14,0},{1,3},{3,5},... | collective-permute-start | bytes 589832 | tf_op jit(solution)/shard_map/ppermute | solution.py:19
  92.8 6.2 %collective-permute-start.14 = (bf16[48,2048]{1,0:T(8,128)(2,1)S(1)}, bf16[48,2048]{1,0:T(8,128)(2,1)S(1)}, u32[]{:S(2)}, u32[]{:S(2)}) collective-permute-start(bf16[48,2048]{1,0:T(8,128)(2,1)S(1)} %reshape.33.refs_4_), channel_id=1, source_target_pairs={{0,14},{2,0},{4,2},{6,4},{8,6},{10,8},{12,10},{14,12},{1,15},{3,1}... | collective-permute-start | bytes 589832 | tf_op jit(solution)/shard_map/ppermute | solution.py:19
  96.3 7.1 %collective-permute-start.18 = (bf16[48,2048]{1,0:T(8,128)(2,1)S(1)}, bf16[48,2048]{1,0:T(8,128)(2,1)S(1)}, u32[]{:S(2)}, u32[]{:S(2)}) collective-permute-start(bf16[48,2048]{1,0:T(8,128)(2,1)S(1)} %collective-permute-done.17.refs_3_), channel_id=1, source_target_pairs={{0,2},{2,4},{4,6},{6,8},{8,10},{10,12},{12,14},{14,0},{1,3},{3,5},... | collective-permute-start | bytes 589832 | tf_op jit(solution)/shard_map/ppermute | solution.py:19
  99.1 7.1 %collective-permute-start.15 = (bf16[48,2048]{1,0:T(8,128)(2,1)S(1)}, bf16[48,2048]{1,0:T(8,128)(2,1)S(1)}, u32[]{:S(2)}, u32[]{:S(2)}) collective-permute-start(bf16[48,2048]{1,0:T(8,128)(2,1)S(1)} %collective-permute-done.14.refs_0_), channel_id=1, source_target_pairs={{0,14},{2,0},{4,2},{6,4},{8,6},{10,8},{12,10},{14,12},{1,15},{3,1}... | collective-permute-start | bytes 589832 | tf_op jit(solution)/shard_map/ppermute | solution.py:19
  103.4 7.6 %collective-permute-start.19 = (bf16[48,2048]{1,0:T(8,128)(2,1)S(1)}, bf16[48,2048]{1,0:T(8,128)(2,1)S(1)}, u32[]{:S(2)}, u32[]{:S(2)}) collective-permute-start(bf16[48,2048]{1,0:T(8,128)(2,1)S(1)} %collective-permute-done.18.refs_6_), channel_id=1, source_target_pairs={{0,2},{2,4},{4,6},{6,8},{8,10},{10,12},{12,14},{14,0},{1,3},{3,5},... | collective-permute-start | bytes 589832 | tf_op jit(solution)/shard_map/ppermute | solution.py:19
  106.2 7.3 %collective-permute-start.16 = (bf16[48,2048]{1,0:T(8,128)(2,1)S(1)}, bf16[48,2048]{1,0:T(8,128)(2,1)S(1)}, u32[]{:S(2)}, u32[]{:S(2)}) collective-permute-start(bf16[48,2048]{1,0:T(8,128)(2,1)S(1)} %collective-permute-done.15.refs_5_), channel_id=1, source_target_pairs={{0,14},{2,0},{4,2},{6,4},{8,6},{10,8},{12,10},{14,12},{1,15},{3,1}... | collective-permute-start | bytes 589832 | tf_op jit(solution)/shard_map/ppermute | solution.py:19
  111.0 6.5 %collective-permute-start.22 = (bf16[48,2048]{1,0:T(8,128)(2,1)S(1)}, bf16[48,2048]{1,0:T(8,128)(2,1)}, u32[]{:S(2)}, u32[]{:S(2)}) collective-permute-start(bf16[48,2048]{1,0:T(8,128)(2,1)S(1)} %collective-permute-done.19.refs_2_), channel_id=1, source_target_pairs={{0,2},{2,4},{4,6},{6,8},{8,10},{10,12},{12,14},{14,0},{1,3},{3,5},... | collective-permute-start | bytes 589832 | tf_op jit(solution)/shard_map/ppermute | solution.py:19
  116.5 0.8 copy-start.3
  117.3 8.8 %collective-permute-start.24 = (bf16[192,512]{1,0:T(8,128)(2,1)}, bf16[192,512]{1,0:T(8,128)(2,1)S(1)}, u32[]{:S(2)}, u32[]{:S(2)}) collective-permute-start(bf16[192,512]{1,0:T(8,128)(2,1)} %get-tuple-element.41), channel_id=1, source_target_pairs={{0,2},{2,0},{4,6},{6,4},{8,10},{10,8},{12,14},{14,12},{1,3},{3,1},... | collective-permute-start | bytes 589832 | tf_op jit(solution)/shard_map/ppermute | solution.py:57
  117.3 0.7 copy-start.14
  118.0 1.1 copy-start.4
  128.2 9.8 %collective-permute-start.27 = (bf16[48,2048]{1,0:T(8,128)(2,1)S(1)}, bf16[48,2048]{1,0:T(8,128)(2,1)S(1)}, u32[]{:S(2)}, u32[]{:S(2)}) collective-permute-start(bf16[48,2048]{1,0:T(8,128)(2,1)S(1)} %get-tuple-element.44), channel_id=1, source_target_pairs={{0,4},{2,6},{4,8},{6,10},{8,12},{10,14},{12,0},{14,2},{1,5},{3,7},... | collective-permute-start | bytes 589832 | tf_op jit(solution)/shard_map/ppermute | solution.py:19
  131.5 7.7 %collective-permute-start.28 = (bf16[48,2048]{1,0:T(8,128)(2,1)S(1)}, bf16[48,2048]{1,0:T(8,128)(2,1)S(1)}, u32[]{:S(2)}, u32[]{:S(2)}) collective-permute-start(bf16[48,2048]{1,0:T(8,128)(2,1)S(1)} %get-tuple-element.45), channel_id=1, source_target_pairs={{0,12},{2,14},{4,0},{6,2},{8,4},{10,6},{12,8},{14,10},{1,13},{3,15... | collective-permute-start | bytes 589832 | tf_op jit(solution)/shard_map/ppermute | solution.py:19
  132.4 12.5 %collective-permute-start.29 = (bf16[48,2048]{1,0:T(8,128)(2,1)S(1)}, bf16[48,2048]{1,0:T(8,128)(2,1)S(1)}, u32[]{:S(2)}, u32[]{:S(2)}) collective-permute-start(bf16[48,2048]{1,0:T(8,128)(2,1)S(1)} %get-tuple-element.46), channel_id=1, source_target_pairs={{0,8},{2,10},{4,12},{6,14},{8,0},{10,2},{12,4},{14,6},{1,9},{3,11}... | collective-permute-start | bytes 589832 | tf_op jit(solution)/shard_map/ppermute | solution.py:19
  156.6 0.9 copy-start.9
  156.6 0.9 copy-start.16
